TPU v7x, 1024 devices: a whole 8x8x8 slice. The times are simulated.
1024 devices in a mesh: ep: 64 (over z, y), tp: 16 (over x, core).
Axes of the slice: x: 8, y: 8, z: 8, core: 2. Of those that a mesh axis runs over, the one named last changes fastest.
Arguments:
- tokens: bfloat16 [8192, 2048], P('ep'), may hold values from -6 to 6
- out_grad: bfloat16 [8192, 2048], P('ep'), may hold values from -50 to 50
- expert_ids: int32 [8192, 2], P('ep'), may hold values from 0 to 63, all different within a row; in each aligned block of 128 rows (0 to 127, 128 to 255, ...) at most 5 rows name the same one
- route_weights: float32 [8192, 2], P('ep'), may hold values from 0.2 to 2
- gate_proj: bfloat16 [64, 2048, 2048], P('ep', 'tp'), may hold values from -0.125 to 0.125
- up_proj: bfloat16 [64, 2048, 2048], P('ep', 'tp'), may hold values from -0.125 to 0.125
- down_proj: bfloat16 [64, 2048, 2048], P('ep', 'tp'), may hold values from -0.125 to 0.125
- shared_act: bfloat16 [8192, 1024], P('ep'), may hold values from -0.29882812 to 0.29882812
Outputs:
- token_grad: bfloat16 [8192, 2048], P('ep', 'tp')
- route_grad: float32 [8192, 2], P('ep')
- gate_grad: bfloat16 [64, 2048, 2048], P('ep', 'tp')
- up_grad: bfloat16 [64, 2048, 2048], P('ep', 'tp')
- down_grad: bfloat16 [64, 2048, 2048], P('ep', 'tp')
- row_norms: float32 [64, 3, 2048], P('ep', None, 'tp')
- shared_grad: float32 [1024, 2048], P('tp', 'ep')
- shared_norms: float32 [1024], P('tp')
Inputs may be any that keep to these rules, and one draw needn't show every extreme that they name: `expert_ids`: each row names 2 different experts. In the rows of one device no expert is named more than 5 times, and in some device some expert is named exactly 5 times.
All inputs are finite; a program needn't handle non-finite values.
Results may differ from a plain program's by a relative error of at most 0.008.
Values may be sent and summed in bfloat16 or wider, within the bound.
No kernel may reach another device: no remote copies, remote signals or barrier semaphores. Data moves between devices by JAX's collectives and lax.ppermute only.
A program may use at most 32 MiB of HBM per device.

v0:
```python
import functools
import math

import jax
import jax.numpy as jnp
from jax import lax
from jax.sharding import Mesh
from jax.sharding import PartitionSpec as P

EP = ("ep_0", "ep_1")


def in_one_piece(arrays, axis, dim, along):
    ends, at = ([], 0)
    for a in arrays[:-1]:
        at += a.shape[along]
        ends.append(at)
    both = jnp.concatenate(arrays, axis=along)
    return tuple(jnp.split(lax.all_gather(both, axis, axis=dim, tiled=True), ends, axis=along))


def side_by_side(arrays, axis, split_dim, concat_dim, along):
    widths = [math.prod(a.shape[along:]) for a in arrays]
    both = jnp.concatenate(
        [a.reshape(*a.shape[:along], w) for a, w in zip(arrays, widths)], axis=along
    )
    filled = lax.all_to_all(both, axis, split_axis=split_dim, concat_axis=concat_dim, tiled=True)
    blocks = jnp.split(filled, [sum(widths[:k]) for k in range(1, len(widths))], axis=along)
    return tuple(
        (b.reshape(*filled.shape[:along], *a.shape[along:]) for a, b in zip(arrays, blocks))
    )


def cut_along(x, dim, length):
    before, after = (x.shape[:dim], x.shape[dim + 1 :])
    return jnp.moveaxis(x.reshape(*before, length, -1, *after), dim, 0)


def sum_at_owner(x, axis, dim):
    length = lax.axis_size(axis)
    blocks = lax.all_to_all(cut_along(x, dim, length), axis, 0, 0, tiled=True)
    return jnp.sum(blocks, axis=0)


def one_axis_at_a_time(x, axes):
    return functools.reduce(lax.psum, axes, x)


def local(tokens, out_grad, expert_ids, route_weights, gate_proj, up_proj, down_proj, shared_act):
    ep_count = lax.axis_size(EP)
    tp_count = lax.axis_size("tp")
    tok_count, model_width = tokens.shape
    top_count = expert_ids.shape[1]
    exp_local = gate_proj.shape[0]
    experts = exp_local * ep_count
    capacity = 5 * tok_count * top_count // (4 * experts)
    slot_count = experts * capacity
    assign = tok_count * top_count
    columns = model_width // tp_count
    offset = lax.axis_index("tp") * columns
    flat_expert = expert_ids.reshape(assign)
    onehot = (flat_expert[:, None] == jnp.arange(experts, dtype=jnp.int32)[None, :]).astype(
        jnp.float32
    )
    earlier = (jnp.arange(assign)[:, None] > jnp.arange(assign)[None, :]).astype(jnp.float32)
    counted = jnp.dot(earlier, onehot, precision=lax.Precision.HIGHEST)
    rank_in = jnp.sum(counted * onehot, 1).astype(jnp.int32)
    slot_id = flat_expert * capacity + rank_in
    picked = (jnp.arange(slot_count, dtype=jnp.int32)[:, None] == slot_id[None, :]).astype(
        jnp.float32
    )
    source_id = jnp.dot(
        picked, jnp.arange(assign, dtype=jnp.float32), precision=lax.Precision.HIGHEST
    ).astype(jnp.int32)
    filled = jnp.sum(picked, 1) > 0.5
    scaled = (
        (route_weights[:, :, None] * out_grad[:, None, :])
        .astype(jnp.bfloat16)
        .reshape(assign, model_width)
    )

    def slot_rows(source_rows, row_index):
        taken = jnp.take(source_rows, row_index, axis=0)
        return jnp.where(filled[:, None], taken, jnp.zeros((), source_rows.dtype))

    token_part = lax.dynamic_slice_in_dim(tokens, offset, columns, 1)
    scaled_part = lax.dynamic_slice_in_dim(scaled, offset, columns, 1)
    send_in = slot_rows(token_part, source_id // top_count).reshape(
        ep_count, exp_local, capacity, columns
    )
    send_cot = slot_rows(scaled_part, source_id).reshape(ep_count, exp_local, capacity, columns)
    part_in, part_cot = (
        lax.all_to_all(send_in, EP, split_axis=0, concat_axis=2, tiled=True),
        lax.all_to_all(send_cot, EP, split_axis=0, concat_axis=2, tiled=True),
    )
    joined_in, joined_cot = in_one_piece((part_in, part_cot), "tp", 3, 0)
    rows_in = joined_in[0]
    rows_cot = joined_cot[0]
    gate_pre = jnp.einsum("erd,efd->erf", rows_in, gate_proj, preferred_element_type=jnp.float32)
    up_pre = jnp.einsum("erd,efd->erf", rows_in, up_proj, preferred_element_type=jnp.float32)
    sigmoid_a = jax.nn.sigmoid(gate_pre)
    silu_a = gate_pre * sigmoid_a
    hidden = (silu_a * up_pre).astype(jnp.bfloat16)
    hidden_grad = jnp.einsum(
        "erd,efd->erf", rows_cot, down_proj, preferred_element_type=jnp.float32
    )
    up_delta = (hidden_grad * silu_a).astype(jnp.bfloat16)
    gate_delta = (hidden_grad * up_pre * sigmoid_a * (1.0 + gate_pre * (1.0 - sigmoid_a))).astype(
        jnp.bfloat16
    )
    gate_full = jnp.einsum("erf,erd->efd", gate_delta, rows_in, preferred_element_type=jnp.float32)
    up_full = jnp.einsum("erf,erd->efd", up_delta, rows_in, preferred_element_type=jnp.float32)
    down_full = jnp.einsum("erf,erd->efd", hidden, rows_cot, preferred_element_type=jnp.float32)
    row_norms = jnp.stack(
        [
            jnp.sum(gate_full * gate_full, 2),
            jnp.sum(up_full * up_full, 2),
            jnp.sum(down_full * down_full, 2),
        ],
        axis=1,
    )
    row_total = rows_in.shape[1]
    partial_value = jnp.einsum(
        "erf,efd->erd", gate_delta, gate_proj, preferred_element_type=jnp.float32
    )
    partial_value = partial_value + jnp.einsum(
        "erf,efd->erd", up_delta, up_proj, preferred_element_type=jnp.float32
    )
    partials = partial_value.astype(jnp.bfloat16).reshape(exp_local, row_total, tp_count, columns)
    inner_part = jnp.sum(hidden.astype(jnp.float32) * hidden_grad, 2).astype(jnp.bfloat16)
    inner_parts = jnp.broadcast_to(inner_part[:, :, None], (exp_local, row_total, tp_count))
    received, received_inner = side_by_side((partials, inner_parts), "tp", 2, 2, 3)
    slot_grad = jnp.sum(received.astype(jnp.float32), 2)
    inner = jnp.sum(received_inner.astype(jnp.float32), 2)
    returned, returned_inner = side_by_side(
        (
            slot_grad.reshape(exp_local, ep_count, capacity, columns),
            inner.reshape(exp_local, ep_count, capacity),
        ),
        EP,
        1,
        0,
        3,
    )
    slot_back = returned.reshape(slot_count, columns)
    inner_back = returned_inner.reshape(slot_count)
    token_grad = jnp.take(slot_back, slot_id, axis=0).reshape(tok_count, top_count, columns).sum(1)
    route_grad = jnp.take(inner_back, slot_id).reshape(tok_count, top_count) / route_weights
    shared_rows = shared_act.shape[1] // tp_count
    shared_part = lax.dynamic_slice_in_dim(
        shared_act, lax.axis_index("tp") * shared_rows, shared_rows, 1
    )
    shared_term = lax.dot_general(
        shared_part, out_grad, (((0,), (0,)), ((), ())), preferred_element_type=jnp.float32
    )
    shared_grad = sum_at_owner(shared_term, EP, 1)
    shared_norms = one_axis_at_a_time(jnp.sum(shared_grad * shared_grad, 1), EP)
    return (
        token_grad.astype(jnp.bfloat16),
        route_grad,
        gate_full.astype(jnp.bfloat16),
        up_full.astype(jnp.bfloat16),
        down_full.astype(jnp.bfloat16),
        row_norms,
        shared_grad,
        shared_norms,
    )


def solution(mesh):
    torus = Mesh(mesh.devices.reshape(8, 8, mesh.shape["tp"]), ("ep_0", "ep_1", "tp"))
    return jax.shard_map(
        local,
        mesh=torus,
        in_specs=(
            P(EP, None),
            P(EP, None),
            P(EP, None),
            P(EP, None),
            P(EP, "tp", None),
            P(EP, "tp", None),
            P(EP, "tp", None),
            P(EP, None),
        ),
        out_specs=(
            P(EP, "tp"),
            P(EP, None),
            P(EP, "tp", None),
            P(EP, "tp", None),
            P(EP, "tp", None),
            P(EP, None, "tp"),
            P("tp", EP),
            P("tp"),
        ),
        check_vma=False,
    )
```

profile of v0, /device:TPU:8, one launch (start us, length us, event | category | flops | bytes accessed | tf_op | source)
XLA Modules:
  0.0 215.6 jit_solution(7292039454010857968)
XLA Ops:
  9.6 1.4 gather_fusion
  12.6 2.1 mul.110
  14.7 2.5 %mul.111 = f32[256,2048]{1,0:T(8,128)} reshape(f32[128,2,2048]{2,1,0:T(2,128)S(1)} %mul.110) | data formatting | bytes 4194304 | tf_op jit(solution)/shard_map/mul | solution.py:77
  18.3 1.4 gather_fusion.1
  21.2 35.9 %all_to_all.46 = bf16[64,1,5,128]{3,2,1,0:T(8,128)(2,1)S(1)} all-to-all(bf16[64,1,5,128]{3,2,1,0:T(8,128)(2,1)S(1)} %get-tuple-element.62), channel_id=1, replica_groups=mesh['ep_0'=8,'ep_1'=8,'tp'=16] {'ep_0','ep_1'}, dimensions={0} | all-to-all | bytes 163840 | tf_op jit(solution)/shard_map/all_to_all | solution.py:93
  57.1 4.6 %all-to-all-start.1 = ((bf16[64,1,5,128]{3,2,1,0:T(8,128)(2,1)}), bf16[64,1,5,128]{3,2,1,0:T(8,128)(2,1)S(1)}, u32[]{:S(2)}, u32[]{:S(2)}) async-start(bf16[64,1,5,128]{3,2,1,0:T(8,128)(2,1)} %get-tuple-element.63), calls=%async_computation.1 | async-start | bytes 262144 | tf_op jit(solution)/shard_map/all_to_all | solution.py:94
  61.8 12.6 %all-to-all-done.1 = bf16[64,1,5,128]{3,2,1,0:T(8,128)(2,1)S(1)} async-done(((bf16[64,1,5,128]{3,2,1,0:T(8,128)(2,1)}), bf16[64,1,5,128]{3,2,1,0:T(8,128)(2,1)S(1)}, u32[]{:S(2)}, u32[]{:S(2)}) %all-to-all-start.1) | async-done | bytes 81952 | tf_op jit(solution)/shard_map/all_to_all | solution.py:94
  76.4 1.4 reshape.336
  77.8 5.6 %all-to-all-start.4 = ((f32[64,1,2048]{2,1,0:T(1,128)}), f32[64,1,2048]{2,1,0:T(1,128)}, u32[]{:S(2)}, u32[]{:S(2)}) async-start(f32[64,1,2048]{2,1,0:T(1,128)} %reshape.336), calls=%async_computation.4 | async-start | bytes 1048576 | tf_op jit(solution)/shard_map/all_to_all | solution.py:41
  83.5 28.6 %all-gather.2.cloned.1.call-done = bf16[2,1,320,2048]{3,2,1,0:T(8,128)(2,1)} async-done(((bf16[2,1,320,128]{3,2,1,0:T(8,128)(2,1)}), bf16[2,1,320,2048]{3,2,1,0:T(8,128)(2,1)}) %all-gather.2.cloned.1.call-update) | async-done | bytes 2621456 | tf_op jit(solution)/shard_map/all_gather | solution.py:19
  112.1 2.0 fusion.6
  114.1 1.8 fusion.7
  119.1 1.4 pad_maximum_fusion
  120.5 7.2 %all-to-all-start.2 = ((bf16[1,320,16,129]{1,3,0,2:T(8,128)(2,1)}), bf16[1,320,16,129]{1,3,0,2:T(8,128)(2,1)S(1)}, u32[]{:S(2)}, u32[]{:S(2)}) async-start(bf16[1,320,16,129]{1,3,0,2:T(8,128)(2,1)} %pad_maximum_fusion), calls=%async_computation.2 | async-start | bytes 3342336 | tf_op jit(solution)/shard_map/all_to_all | solution.py:27
  129.8 3.7 %reduce.15 = f32[64,2048]{1,0:T(8,128)} reduce(f32[64,1,2048]{2,1,0:T(1,128)} %all-to-all-done.4, f32[]{:T(128)} %broadcast.184), dimensions={1}, to_apply=%all_to_all.40.reduce_sub_computation | reduce | bytes 1048580 | tf_op jit(solution)/shard_map/all_to_all | solution.py:41
  133.5 1.5 reshape.337
  135.1 19.6 %psum.14 = f32[64]{0:T(128)S(1)} all-reduce(f32[64]{0:T(128)S(1)} %multiply_reduce_fusion.4), channel_id=1, replica_groups=mesh['ep_0'=8,'ep_1'=8,'tp'=16] {'ep_0'}, use_global_device_ids=true, to_apply=%region_11.12 | all-reduce | flops 64 | bytes 512 | tf_op jit(solution)/shard_map/psum | solution.py:46
  154.7 17.6 %psum.15 = f32[64]{0:T(128)} all-reduce(f32[64]{0:T(128)S(1)} %psum.14), channel_id=1, replica_groups=mesh['ep_0'=8,'ep_1'=8,'tp'=16] {'ep_1'}, use_global_device_ids=true, to_apply=%region_12.13 | all-reduce | flops 64 | bytes 512 | tf_op jit(solution)/shard_map/psum | solution.py:46
  172.3 3.1 %multiply_reduce_fusion.2 = (f32[128]{0:T(128)}, bf16[1,128,2048]{2,1,0:T(8,128)(2,1)}) fusion(bf16[320,128]{1,0:T(8,128)(2,1)S(1)} %copy-done.8, bf16[2,1,320,2048]{3,2,1,0:T(8,128)(2,1)} %all-gather.2.cloned.1.call-done), kind=kOutput, calls=%fused_computation.17 | convolution fusion | flops 168558464 | bytes 1917440 | tf_op jit(solution)/shard_map/erf,erd->efd/dot_general | solution.py:111
  175.4 2.8 %fusion.1 = f32[128,2048]{1,0:T(8,128)} fusion(bf16[320,128]{1,0:T(8,128)(2,1)S(1)} %copy-done.11, bf16[2,1,320,2048]{3,2,1,0:T(8,128)(2,1)} %all-gather.2.cloned.1.call-done), kind=kOutput, calls=%fused_computation.10 | convolution fusion | flops 167772160 | bytes 2441216 | tf_op jit(solution)/shard_map/erf,erd->efd/dot_general | solution.py:113
  181.7 7.7 %all-to-all-start.3 = ((f32[1,64,5,129]{3,0,2,1:T(1,128)}), f32[1,64,5,129]{3,0,2,1:T(1,128)S(1)}, u32[]{:S(2)}, u32[]{:S(2)}) async-start(f32[1,64,5,129]{3,0,2,1:T(1,128)} %copy.59), calls=%async_computation.3 | async-start | bytes 655360 | tf_op jit(solution)/shard_map/all_to_all | solution.py:27
  189.4 3.0 %multiply_reduce_fusion = (f32[128]{0:T(128)S(1)}, bf16[1,128,2048]{2,1,0:T(8,128)(2,1)}, bf16[1,128,2048]{2,1,0:T(8,128)(2,1)}, f32[128]{0:T(128)S(1)}) fusion(f32[128,2048]{1,0:T(8,128)} %fusion.1, bf16[320,128]{1,0:T(8,128)(2,1)} %copy-done.9, bf16[2,1,320,2048]{3,2,1,0:T(8,128)(2,1)S(1)} %copy-done.2), kind=kOutput, calls=%fused_computation.15 | convolution fusion | flops 169344768 | bytes 3490816 | tf_op jit(solution)/shard_map/erf,erd->efd/dot_general | solution.py:112
  193.0 10.4 %all-to-all-done.3 = f32[1,64,5,129]{3,0,2,1:T(1,128)S(1)} async-done(((f32[1,64,5,129]{3,0,2,1:T(1,128)}), f32[1,64,5,129]{3,0,2,1:T(1,128)S(1)}, u32[]{:S(2)}, u32[]{:S(2)}) %all-to-all-start.3) | async-done | bytes 165152 | tf_op jit(solution)/shard_map/all_to_all | solution.py:27
  204.3 1.9 gather_fusion.3
  (92 shorter events, 21.2 us)
Async XLA Ops:
  7.2 104.9 %copy-start = (bf16[1,128,2048]{2,1,0:T(8,128)(2,1)S(1)}, bf16[1,128,2048]{2,1,0:T(8,128)(2,1)}, u32[]{:S(2)}) copy-start(bf16[1,128,2048]{2,1,0:T(8,128)(2,1)} %param.12) | copy-start | bytes 1572868
  11.9 0.6 copy-start.4
  17.2 58.0 %copy-start.3 = (bf16[128,2048]{1,0:T(8,128)(2,1)S(1)}, bf16[128,2048]{1,0:T(8,128)(2,1)}, u32[]{:S(2)}) copy-start(bf16[128,2048]{1,0:T(8,128)(2,1)} %param.9) | copy-start | bytes 1572868
  57.1 17.4 %all-to-all-start.1 = ((bf16[64,1,5,128]{3,2,1,0:T(8,128)(2,1)}), bf16[64,1,5,128]{3,2,1,0:T(8,128)(2,1)S(1)}, u32[]{:S(2)}, u32[]{:S(2)}) async-start(bf16[64,1,5,128]{3,2,1,0:T(8,128)(2,1)} %get-tuple-element.63), calls=%async_computation.1 | async-start | bytes 262144 | tf_op jit(solution)/shard_map/all_to_all | solution.py:94
  61.7 50.4 %all-gather.2.cloned.1.call-start = ((), (), s32[]{:S(2)}) async-start(), calls=%async_computation.5 | async-start | bytes 2785280 | tf_op jit(solution)/shard_map/all_gather | solution.py:19
  77.8 36.3 %copy-start.6 = (bf16[1,128,2048]{2,1,0:T(8,128)(2,1)S(1)}, bf16[1,128,2048]{2,1,0:T(8,128)(2,1)}, u32[]{:S(2)}) copy-start(bf16[1,128,2048]{2,1,0:T(8,128)(2,1)} %param.13) | copy-start | bytes 1572868
  77.8 42.7 %all-to-all-start.4 = ((f32[64,1,2048]{2,1,0:T(1,128)}), f32[64,1,2048]{2,1,0:T(1,128)}, u32[]{:S(2)}, u32[]{:S(2)}) async-start(f32[64,1,2048]{2,1,0:T(1,128)} %reshape.336), calls=%async_computation.4 | async-start | bytes 1048576 | tf_op jit(solution)/shard_map/all_to_all | solution.py:41
  83.5 32.5 %copy-start.15 = (bf16[1,128,2048]{2,1,0:T(8,128)(2,1)S(1)}, bf16[1,128,2048]{2,1,0:T(8,128)(2,1)}, u32[]{:S(2)}) copy-start(bf16[1,128,2048]{2,1,0:T(8,128)(2,1)} %param.14) | copy-start | bytes 1572868
  112.1 3.8 %copy-start.1 = (bf16[2,1,320,2048]{3,2,1,0:T(8,128)(2,1)S(1)}, bf16[2,1,320,2048]{3,2,1,0:T(8,128)(2,1)}, u32[]{:S(2)}) copy-start(bf16[2,1,320,2048]{3,2,1,0:T(8,128)(2,1)} %all-gather.2.cloned.1.call-done) | copy-start | bytes 7864324
  117.1 0.6 copy-start.7
  117.1 0.7 copy-start.9
  120.5 57.7 %all-to-all-start.2 = ((bf16[1,320,16,129]{1,3,0,2:T(8,128)(2,1)}), bf16[1,320,16,129]{1,3,0,2:T(8,128)(2,1)S(1)}, u32[]{:S(2)}, u32[]{:S(2)}) async-start(bf16[1,320,16,129]{1,3,0,2:T(8,128)(2,1)} %pad_maximum_fusion), calls=%async_computation.2 | async-start | bytes 3342336 | tf_op jit(solution)/shard_map/all_to_all | solution.py:27
  127.7 44.6 %copy-start.8 = (bf16[320,128]{1,0:T(8,128)(2,1)S(1)}, bf16[320,128]{1,0:T(8,128)(2,1)}, u32[]{:S(2)}) copy-start(bf16[320,128]{1,0:T(8,128)(2,1)} %copy-done.7) | copy-start | bytes 245764
  133.5 41.9 %copy-start.11 = (bf16[320,128]{1,0:T(8,128)(2,1)S(1)}, bf16[320,128]{1,0:T(8,128)(2,1)}, u32[]{:S(2)}) copy-start(bf16[320,128]{1,0:T(8,128)(2,1)} %get-tuple-element.51) | copy-start | bytes 245764
  135.1 43.1 %copy-start.12 = (f32[64,32]{0,1:T(8,128)}, f32[64,32]{0,1:T(8,128)S(1)}, u32[]{:S(2)}) copy-start(f32[64,32]{0,1:T(8,128)S(1)} %bitcast_reduce_fusion) | copy-start | bytes 24580
  179.3 10.1 %copy-start.2 = (bf16[2,1,320,2048]{3,2,1,0:T(8,128)(2,1)S(1)}, bf16[2,1,320,2048]{3,2,1,0:T(8,128)(2,1)}, u32[]{:S(2)}) copy-start(bf16[2,1,320,2048]{3,2,1,0:T(8,128)(2,1)} %all-gather.2.cloned.1.call-done) | copy-start | bytes 7864324
  181.7 10.7 %copy-start.14 = (f32[128]{0:T(128)S(1)}, f32[128]{0:T(128)}, u32[]{:S(2)}) copy-start(f32[128]{0:T(128)} %get-tuple-element.54) | copy-start | bytes 1540
  181.7 21.7 %all-to-all-start.3 = ((f32[1,64,5,129]{3,0,2,1:T(1,128)}), f32[1,64,5,129]{3,0,2,1:T(1,128)S(1)}, u32[]{:S(2)}, u32[]{:S(2)}) async-start(f32[1,64,5,129]{3,0,2,1:T(1,128)} %copy.59), calls=%async_computation.3 | async-start | bytes 655360 | tf_op jit(solution)/shard_map/all_to_all | solution.py:27
  189.4 14.9 %copy-start.13 = (s32[1024]{0:T(1024)S(1)}, s32[1024]{0:T(1024)}, u32[]{:S(2)}) copy-start(s32[1024]{0:T(1024)} %pad_clamp_fusion) | copy-start | bytes 12292
  192.5 14.7 %copy-start.5 = (f32[128,2]{1,0:T(8,128)S(1)}, f32[128,2]{1,0:T(8,128)}, u32[]{:S(2)}) copy-start(f32[128,2]{1,0:T(8,128)} %copy-done.4) | copy-start | bytes 3076
  192.5 14.7 %copy-start.10 = (s32[128,2]{1,0:T(8,128)S(1)}, s32[128,2]{1,0:T(8,128)}, u32[]{:S(2)}) copy-start(s32[128,2]{1,0:T(8,128)} %convert_element_type.106) | copy-start | bytes 3076
Sparse Core Ops, SparseCore 0:
  75.3 36.6 all-gather.1
where the time goes:
time: 217 us; the launch traced here: 216 us
  blocking collectives  73.1 us (34%)
  waiting for transfers between devices  51.7 us (24%)
  starting transfers between devices  25.2 us (12%)
  local copies, waits for them, and re-layouts  23.7 us (11%)
  matrix products  16.4 us (8%)
  between operations  14.4 us (7%)
  other arithmetic  11.1 us (5%)
    psum x2, blocking collectives, one_axis_at_a_time(): return functools.reduce(lax.psum, axes, x)  37.2 us
    all_to_all x1, blocking collectives, local(): lax.all_to_all(send_in, EP, split_axis=0, concat_axis=2, tiled=True)  35.9 us
    all_gather x1, waiting for transfers between devices, in_one_piece(): lax.all_gather(both, axis, axis=dim, tiled=True)  28.6 us
    all_to_all x2, starting transfers between devices, side_by_side(): lax.all_to_all(both, axis, split_axis=split_dim, concat_axis=concat_dim,...  14.9 us
    all_to_all x1, waiting for transfers between devices, local(): lax.all_to_all(send_cot, EP, split_axis=0, concat_axis=2, tiled=True)  12.6 us
    all_to_all x2, waiting for transfers between devices, side_by_side(): lax.all_to_all(both, axis, split_axis=split_dim, concat_axis=concat_dim,...  10.4 us
    unnamed x38, local copies, waits for them, and re-layouts  6.61 us
    all_to_all x1, starting transfers between devices, sum_at_owner(): blocks = lax.all_to_all(cut_along(x, dim, length), axis, 0, 0, tiled=True)  5.63 us
  transfers between devices with their start and end apart: 5, of which 3 were waited for; matrix products, arithmetic and copies ran while one was open for 13% of the time, Pallas kernels for 0%

commit v1 on v0

v1 whole, which is shorter than its diff:
```python
import functools

import jax
import jax.numpy as jnp
from jax import lax
from jax.experimental import pallas as pl
from jax.experimental.pallas import tpu as pltpu
from jax.sharding import Mesh
from jax.sharding import PartitionSpec as P

EP = ("z", "y")
TP = ("x", "c")
BF, F32, I32 = jnp.bfloat16, jnp.float32, jnp.int32
LANES = 128
TILE = 8
HALF = TILE * LANES
SHARED = 2


def params(mib):
    return pltpu.CompilerParams(vmem_limit_bytes=mib * 1024 * 1024)


def in_vmem(n):
    return [pl.BlockSpec(memory_space=pltpu.VMEM)] * n


def in_smem(n):
    return [pl.BlockSpec(memory_space=pltpu.SMEM)] * n


def iota(shape, dim):
    return lax.broadcasted_iota(I32, shape, dim)


def ones_at(mask):
    return mask.astype(F32).astype(BF)


def dot(a, b, ca=1, cb=0):
    return lax.dot_general(a, b, (((ca,), (cb,)), ((), ())), preferred_element_type=F32)


def split2(v):
    hi = v.astype(BF).astype(F32)
    return hi, v - hi


def spread(ref, x):
    for j in range(TILE):
        cols = x[:, j * LANES : (j + 1) * LANES].astype(F32)
        ref[pl.ds(j, x.shape[0], stride=TILE), :] = cols


def gather_cols(ref, count, j):
    return ref[pl.ds(j, count, stride=TILE), :]


def send_kernel(
    cap, ids_s, w_s, at_s, tok_ref, grad_ref, act_ref, out_ref, rank_s, seen_s, tok_t, grad_t
):
    count, width = grad_ref.shape
    experts = out_ref.shape[0]
    mine = pl.ds(pl.multiple_of((at_s[0] % 2) * HALF, HALF), HALF)
    spread(tok_t, tok_ref[:, mine])
    spread(grad_t, grad_ref[:, mine])
    for e in range(experts):
        seen_s[e] = 0
    out_ref[:, : 2 * cap] = jnp.zeros((experts, 2 * cap, TILE, LANES), BF)

    def one_token(t, carry):
        rows = pl.ds(pl.multiple_of(t * TILE, TILE), TILE)
        tok = tok_t[rows, :].astype(BF)
        grad = grad_t[rows, :]
        for k in range(2):
            e = ids_s[k, t]
            r = seen_s[e]
            seen_s[e] = r + 1
            rank_s[k, t] = r
            out_ref[e, r] = tok
            out_ref[e, cap + r] = (w_s[k, t] * grad).astype(BF)
        return carry

    lax.fori_loop(0, count, one_token, 0, unroll=8)

    half = LANES // 2
    act = act_ref[:, pl.ds(pl.multiple_of((at_s[0] // 2) * LANES, LANES), LANES)]
    swapped = jnp.concatenate([act[:, half:], act[:, :half]], axis=1)
    left = iota(act.shape, 1) < half
    own = (at_s[0] % 2) * half
    keep = (iota(act.shape, 1) // half) * half == own
    twice = jnp.where(keep, act.astype(F32), swapped.astype(F32)).astype(BF)
    step = 2 * LANES
    block = width // experts
    for s in range(0, width, step):
        term = dot(grad_ref[:, s : s + step], twice, 0, 0)
        term = term.reshape(step // block, 2, block // 2, LANES)
        lane = iota((step // block, block // 2, LANES), 2)
        both = jnp.where(lane < half, term[:, 0], term[:, 1]).astype(BF)
        out_ref[s // block : (s + step) // block, 2 * cap :] = both.reshape(
            step // block, SHARED, TILE, LANES
        )


def send_rows(ids_t, w_t, at, tokens, out_grad, act, cap, experts):
    count = tokens.shape[0]
    return pl.pallas_call(
        functools.partial(send_kernel, cap),
        in_specs=in_smem(3) + in_vmem(3),
        out_specs=in_vmem(1) + in_smem(1),
        out_shape=[
            jax.ShapeDtypeStruct((experts, 2 * cap + SHARED, TILE, LANES), BF),
            jax.ShapeDtypeStruct((2, count), I32),
        ],
        scratch_shapes=[
            pltpu.SMEM((experts,), I32),
            pltpu.VMEM((count * TILE, LANES), F32),
            pltpu.VMEM((count * TILE, LANES), F32),
        ],
        compiler_params=params(16),
        name="send_rows",
    )(ids_t, w_t, at, tokens, out_grad, act)


def unpack_kernel(cap, recv_ref, rows_ref, in_t, cot_t):
    n = recv_ref.shape[0]
    count = n * cap
    for k, ref in enumerate((in_t, cot_t)):
        tiles = recv_ref[:, k * cap : (k + 1) * cap].astype(F32)
        ref[...] = tiles.reshape(count * TILE, LANES)
        for j in range(TILE):
            cols = slice(j * LANES, (j + 1) * LANES)
            rows_ref[k, :, cols] = gather_cols(ref, count, j).astype(BF)


def unpack(recv, cap):
    count = recv.shape[0] * cap
    return pl.pallas_call(
        functools.partial(unpack_kernel, cap),
        in_specs=in_vmem(1),
        out_specs=pl.BlockSpec(memory_space=pltpu.VMEM),
        out_shape=jax.ShapeDtypeStruct((2, count, HALF), BF),
        scratch_shapes=[pltpu.VMEM((count * TILE, LANES), F32)] * 2,
        compiler_params=params(16),
        name="unpack",
    )(recv)


def shared_kernel(cap, recv_ref, out_ref, norm_ref):
    n = recv_ref.shape[0]
    total = jnp.sum(recv_ref[:, 2 * cap :].astype(F32), axis=0).reshape(SHARED * TILE, LANES)
    half = LANES // 2
    out_ref[...] = jnp.concatenate([total[:, :half], total[:, half:]], axis=0)
    sq = jnp.sum(total * total, axis=0, keepdims=True)
    sq = sq + jnp.concatenate([sq[:, half:], sq[:, :half]], axis=1)
    norm_ref[...] = jnp.broadcast_to(sq, norm_ref.shape)


def shared_sum(recv, cap):
    return pl.pallas_call(
        functools.partial(shared_kernel, cap),
        in_specs=in_vmem(1),
        out_specs=in_vmem(2),
        out_shape=[
            jax.ShapeDtypeStruct((2 * SHARED * TILE, LANES // 2), F32),
            jax.ShapeDtypeStruct((TILE, LANES), F32),
        ],
        compiler_params=params(16),
        name="shared_sum",
    )(recv)


def forward_kernel(core_s, own_ref, other_ref, gate_ref, up_ref, down_ref, keep_ref, give_ref, delta_ref):
    core = core_s[0]
    count = own_ref.shape[1]
    gate_pre = up_pre = hidden_grad = 0.0
    step = 2 * LANES
    for side, ref in ((core, own_ref), (1 - core, other_ref)):
        for s in range(0, HALF, step):
            cols = pl.ds(pl.multiple_of(side * HALF + s, step), step)
            a, b = ref[0, :, s : s + step], ref[1, :, s : s + step]
            gate_pre = gate_pre + dot(a, gate_ref[0, :, cols], 1, 1)
            up_pre = up_pre + dot(a, up_ref[0, :, cols], 1, 1)
            hidden_grad = hidden_grad + dot(b, down_ref[0, :, cols], 1, 1)
    sig = jax.nn.sigmoid(gate_pre)
    silu = gate_pre * sig
    hidden = (silu * up_pre).astype(BF)
    up_delta = (hidden_grad * silu).astype(BF)
    gate_delta = (hidden_grad * up_pre * sig * (1.0 + gate_pre * (1.0 - sig))).astype(BF)
    both = jnp.concatenate([gate_delta, up_delta], axis=1)
    for ref, side in ((give_ref, 1 - core), (keep_ref, core)):
        for j in range(TILE):
            cols = pl.ds(pl.multiple_of(j * step + side * LANES, LANES), LANES)
            w = jnp.concatenate([gate_ref[0, :, cols], up_ref[0, :, cols]], axis=0)
            ref[:count, j * LANES : (j + 1) * LANES] = dot(both, w).astype(BF)
    for k, d in enumerate((gate_delta, up_delta, hidden)):
        delta_ref[k] = d.astype(F32).T.astype(BF)
    inner = jnp.sum(hidden.astype(F32) * hidden_grad, axis=1, keepdims=True)
    spot = iota((count, LANES), 0) % LANES == iota((count, LANES), 1)
    spots = jnp.where(spot, inner, 0.0)
    lines = [
        jnp.sum(spots[s : min(s + LANES, count)], axis=0, keepdims=True)
        for s in range(0, count, LANES)
    ]
    hi, lo = split2(jnp.concatenate(lines, axis=0))
    pad = jnp.zeros((TILE - 2 * len(lines), LANES), F32)
    tile = jnp.concatenate([hi, lo, pad], axis=0).astype(BF)
    for ref in (keep_ref, give_ref):
        ref[count:, :] = jnp.zeros((TILE, HALF), BF)
        ref[count:, :LANES] = tile


def forward(core, own, other, gate, up, down):
    count = own.shape[1]
    part = jax.ShapeDtypeStruct((count + TILE, HALF), BF)
    return pl.pallas_call(
        forward_kernel,
        in_specs=in_smem(1) + in_vmem(5),
        out_specs=in_vmem(3),
        out_shape=[part, part, jax.ShapeDtypeStruct((3, gate.shape[1], count), BF)],
        compiler_params=params(24),
        name="forward",
    )(core, own, other, gate, up, down)


def grads_kernel(core_s, delta_ref, own_ref, other_ref, gate_ref, up_ref, down_ref, norm_ref):
    core = core_s[0]
    step = 2 * LANES
    norms = []
    for k, (out, which) in enumerate(((gate_ref, 0), (up_ref, 0), (down_ref, 1))):
        total = 0.0
        for side, ref in ((core, own_ref), (1 - core, other_ref)):
            for s in range(0, HALF, step):
                g = dot(delta_ref[k], ref[which, :, s : s + step])
                cols = pl.ds(pl.multiple_of(side * HALF + s, step), step)
                out[0, :, cols] = g.astype(BF)
                sq = g * g
                total = total + sq[:, :LANES] + sq[:, LANES:]
        norms.append(jnp.sum(total.T, axis=0, keepdims=True))
    norm_ref[...] = jnp.concatenate(norms, axis=0)


def grads(core, delta, own, other):
    feats = delta.shape[1]
    out = jax.ShapeDtypeStruct((1, feats, 2 * HALF), BF)
    return pl.pallas_call(
        grads_kernel,
        in_specs=in_smem(1) + in_vmem(3),
        out_specs=in_vmem(4),
        out_shape=[out, out, out, jax.ShapeDtypeStruct((3, feats), F32)],
        compiler_params=params(24),
        name="grads",
    )(core, delta, own, other)


def back_kernel(cap, keep_ref, take_ref, norm_ref, out_ref, tiles):
    n = out_ref.shape[0]
    count = n * cap
    for j in range(TILE):
        cols = slice(j * LANES, (j + 1) * LANES)
        both = keep_ref[:count, cols].astype(F32) + take_ref[:count, cols].astype(F32)
        tiles[pl.ds(j, count, stride=TILE), :] = both
    out_ref[:, :cap] = tiles[...].astype(BF).reshape(n, cap, TILE, LANES)
    both = keep_ref[count:, :LANES].astype(F32) + take_ref[count:, :LANES].astype(F32)
    lines = -(-count // LANES)
    hi, lo = split2(both[:lines] + both[lines : 2 * lines])
    norm_hi, norm_lo = split2(norm_ref[:1])
    norm = jnp.where(iota((1, LANES), 1) < LANES // 2, norm_hi, norm_lo)
    pad = jnp.zeros((TILE - 2 * lines - 1, LANES), F32)
    tile = jnp.concatenate([hi, lo, norm, pad], axis=0).astype(BF)
    out_ref[:, cap] = jnp.broadcast_to(tile[None], (n, TILE, LANES))


def back_rows(keep, take, norms, n, cap):
    return pl.pallas_call(
        functools.partial(back_kernel, cap),
        in_specs=in_vmem(3),
        out_specs=pl.BlockSpec(memory_space=pltpu.VMEM),
        out_shape=jax.ShapeDtypeStruct((n, cap + 1, TILE, LANES), BF),
        scratch_shapes=[pltpu.VMEM((n * cap * TILE, LANES), F32)],
        compiler_params=params(16),
        name="back_rows",
    )(keep, take, norms)


def combine_kernel(cap, ids_s, rank_s, me_s, recv_ref, ids_ref, rank_ref, out_ref, norm_ref, tiles):
    n = recv_ref.shape[0]
    count = ids_ref.shape[1]

    def one_token(t, carry):
        pair = [recv_ref[ids_s[k, t], rank_s[k, t]].astype(F32) for k in range(2)]
        tiles[pl.ds(pl.multiple_of(t * TILE, TILE), TILE), :] = pair[0] + pair[1]
        return carry

    lax.fori_loop(0, count, one_token, 0, unroll=8)
    for j in range(TILE):
        out_ref[j, :count] = gather_cols(tiles, count, j).astype(BF)
    extra = recv_ref[:, cap].reshape(n * TILE, LANES)
    lines = -(-n * cap // LANES)
    o = iota((n * TILE, count), 0)
    route = []
    for k in range(2):
        slot = me_s[0] * cap + rank_ref[k : k + 1, :]
        first = ids_ref[k : k + 1, :] * TILE + slot // LANES
        got = dot(extra, ones_at((o == first) | (o == first + lines)), 0, 0)
        use = iota((LANES, count), 0) == slot % LANES
        route.append(jnp.sum(jnp.where(use, got, 0.0), axis=0, keepdims=True))
    hi, lo = split2(jnp.concatenate(route, axis=0))
    tile = jnp.concatenate([hi, lo, jnp.zeros((TILE - 4, count), F32)], axis=0).astype(BF)
    out_ref[:, count:] = jnp.broadcast_to(tile[None], (TILE, TILE, LANES))
    sums = dot(ones_at(iota((TILE, n * TILE), 1) % TILE == 2 * lines), extra)
    norm_ref[...] = sums[:, : LANES // 2] + sums[:, LANES // 2 :]


def combine(ids_t, rank, me, recv, cap):
    count = ids_t.shape[1]
    return pl.pallas_call(
        functools.partial(combine_kernel, cap),
        in_specs=in_smem(3) + in_vmem(3),
        out_specs=in_vmem(2),
        out_shape=[
            jax.ShapeDtypeStruct((TILE, count + TILE, LANES), BF),
            jax.ShapeDtypeStruct((TILE, LANES // 2), F32),
        ],
        scratch_shapes=[pltpu.VMEM((count * TILE, LANES), F32)],
        compiler_params=params(16),
        name="combine",
    )(ids_t, rank, me, recv, ids_t, rank)


def end_kernel(recv_ref, w_ref, tok_ref, route_ref):
    count = tok_ref.shape[0]
    total = recv_ref[0].astype(F32)
    for x in range(1, recv_ref.shape[0]):
        total = total + recv_ref[x].astype(F32)
    tok_ref[...] = total[:count].astype(BF)
    route_ref[...] = (total[count : count + 2] + total[count + 2 : count + 4]) / w_ref[...]


def end(recv, w_t):
    count = w_t.shape[1]
    return pl.pallas_call(
        end_kernel,
        in_specs=in_vmem(2),
        out_specs=in_vmem(2),
        out_shape=[
            jax.ShapeDtypeStruct((count, LANES), BF),
            jax.ShapeDtypeStruct((2, count), F32),
        ],
        compiler_params=params(16),
        name="end",
    )(recv, w_t)


def swap(v):
    return lax.ppermute(v, "c", [(0, 1), (1, 0)])


def local(tokens, out_grad, expert_ids, route_weights, gate_proj, up_proj, down_proj, shared_act):
    n = lax.axis_size(EP)
    cap = 5 * tokens.shape[0] * expert_ids.shape[1] // (4 * n)
    core = lax.axis_index("c").reshape(1)
    at = lax.axis_index(TP).reshape(1)
    me = lax.axis_index(EP).reshape(1)
    ids_t, w_t = expert_ids.T, route_weights.T
    sent, rank = send_rows(ids_t, w_t, at, tokens, out_grad, shared_act, cap, n)
    recv = lax.all_to_all(sent, EP, 0, 0, tiled=True)
    own = unpack(recv, cap)
    other = swap(own)
    shared, norms = shared_sum(recv, cap)
    keep, give, delta = forward(core, own, other, gate_proj, up_proj, down_proj)
    back = back_rows(keep, swap(give), norms, n, cap)
    returned = lax.all_to_all(back, EP, 0, 0, tiled=True)
    gate_grad, up_grad, down_grad, row_norms = grads(core, delta, own, other)
    parts, shared_norms = combine(ids_t, rank, me, returned, cap)
    summed = lax.all_to_all(parts, "x", 0, 0, tiled=True)
    token_grad, route_grad = end(summed, w_t)
    return (
        token_grad,
        route_grad.T,
        gate_grad,
        up_grad,
        down_grad,
        row_norms[None],
        shared.T,
        shared_norms[0],
    )


def solution(mesh):
    torus = Mesh(mesh.devices.reshape(8, 8, mesh.shape["tp"] // 2, 2), (*EP, *TP))
    return jax.shard_map(
        local,
        mesh=torus,
        in_specs=(
            P(EP, None),
            P(EP, None),
            P(EP, None),
            P(EP, None),
            P(EP, TP, None),
            P(EP, TP, None),
            P(EP, TP, None),
            P(EP, None),
        ),
        out_specs=(
            P(EP, TP),
            P(EP, None),
            P(EP, TP, None),
            P(EP, TP, None),
            P(EP, TP, None),
            P(EP, None, TP),
            P(TP, EP),
            P(TP),
        ),
        check_vma=False,
    )
```

time: 217 us -> 139 us (0.64)
  the two profiles are of different devices: /device:TPU:8 before, /device:TPU:1 now
where the time goes in v1:
time: 139 us; the launch traced here: 136 us
  blocking collectives  62.8 us (45%)
  waiting for transfers between devices  31.9 us (23%)
  starting transfers between devices  21.1 us (15%)
  Pallas kernels  11.7 us (8%)
  local copies, waits for them, and re-layouts  8.02 us (6%)
    all_to_all x1, blocking collectives, local(): recv = lax.all_to_all(sent, EP, 0, 0, tiled=True)  62.8 us
    all_to_all x1, waiting for transfers between devices, local(): returned = lax.all_to_all(back, EP, 0, 0, tiled=True)  22.6 us
    unnamed x29, local copies, waits for them, and re-layouts  7.51 us
    ppermute x2, starting transfers between devices, swap(): return lax.ppermute(v, 'c', [(0, 1), (1, 0)])  7.38 us
    all_to_all x1, starting transfers between devices, local(): returned = lax.all_to_all(back, EP, 0, 0, tiled=True)  7.26 us
    all_to_all x1, starting transfers between devices, local(): summed = lax.all_to_all(parts, 'x', 0, 0, tiled=True)  6.48 us
    all_to_all x1, waiting for transfers between devices, local(): summed = lax.all_to_all(parts, 'x', 0, 0, tiled=True)  5.71 us
    ppermute x2, waiting for transfers between devices, swap(): return lax.ppermute(v, 'c', [(0, 1), (1, 0)])  3.61 us
  transfers between devices with their start and end apart: 4, of which 4 were waited for; matrix products, arithmetic and copies ran while one was open for 1% of the time, Pallas kernels for 2%

profile of v1, /device:TPU:1, one launch (start us, length us, event | category | flops | bytes accessed | tf_op | source)
XLA Modules:
  0.0 136.3 jit_solution(13335087089070577138)
XLA Ops:
  0.7 1.0 copy-done.4
  1.7 1.0 copy-done.5
  2.7 0.9 copy-done.9
  3.7 0.7 copy-done.10
  4.4 0.7 copy-done.12
  5.0 2.7 %send_rows.1 = (bf16[64,12,8,128]{3,2,1,0:T(8,128)(2,1)S(1)}, s32[2,128]{1,0:T(2,128)S(1)}) custom-call(s32[2,128]{1,0:T(2,128)S(1)} %bitcast.10, f32[2,128]{1,0:T(2,128)S(1)} %bitcast.13, s32[1]{0:T(128)} %bitcast.2.at_s, bf16[128,2048]{1,0:T(8,128)(2,1)S(1)} %copy-done.4, bf16[128,2048]{1,0:T(8,128)(2,1)S(1)} %copy-done.5, bf16[128,1024]{1,0:T(8,128)(2,1)S(1)} %copy-done.9), custom_call_target="tpu_custom_call" | custom-call | tf_op jit(solution)/shard_map/send_rows/pallas_call | solution.py:107
  7.8 62.8 %all_to_all.15.recv_ref = bf16[64,12,8,128]{3,2,1,0:T(8,128)(2,1)S(1)} all-to-all(bf16[64,12,8,128]{3,2,1,0:T(8,128)(2,1)S(1)} %get-tuple-element.24), channel_id=1, replica_groups=mesh['z'=8,'y'=8,'x'=8,'c'=2] {'z','y'}, dimensions={0} | all-to-all | bytes 3145728 | tf_op jit(solution)/shard_map/all_to_all | solution.py:367
  70.6 0.7 unpack.1.own_ref
  71.3 5.1 %collective-permute-start = (bf16[2,320,1024]{2,1,0:T(8,128)(2,1)S(1)}, bf16[2,320,1024]{2,1,0:T(8,128)(2,1)S(1)}, u32[]{:S(2)}, u32[]{:S(2)}) collective-permute-start(bf16[2,320,1024]{2,1,0:T(8,128)(2,1)S(1)} %unpack.1.own_ref), channel_id=1, source_target_pairs={{0,1},{1,0},{2,3},{3,2},{4,5},{5,4},{6,7},{7,6},{8,9},{9,8},{10,11... | collective-permute-start | bytes 3932168 | tf_op jit(solution)/shard_map/ppermute | solution.py:356
  76.4 2.6 %collective-permute-done.other_ref = bf16[2,320,1024]{2,1,0:T(8,128)(2,1)S(1)} collective-permute-done((bf16[2,320,1024]{2,1,0:T(8,128)(2,1)S(1)}, bf16[2,320,1024]{2,1,0:T(8,128)(2,1)S(1)}, u32[]{:S(2)}, u32[]{:S(2)}) %collective-permute-start) | collective-permute-done | bytes 1310752 | tf_op jit(solution)/shard_map/ppermute | solution.py:356
  79.1 2.6 %forward.1 = (bf16[328,1024]{1,0:T(8,128)(2,1)S(1)}, bf16[328,1024]{1,0:T(8,128)(2,1)S(1)}, bf16[3,128,320]{2,1,0:T(8,128)(2,1)S(1)}) custom-call(s32[1]{0:T(128)} %bitcast.4.core_s, bf16[2,320,1024]{2,1,0:T(8,128)(2,1)S(1)} %unpack.1.own_ref, bf16[2,320,1024]{2,1,0:T(8,128)(2,1)S(1)} %collective-permute-done.other_ref, bf16[1,128,2048]{2,1,0:T(8,128)(2,1)S(1)} %copy-done.1, ...), custom_call_target="tpu_custom_call" | custom-call | tf_op jit(solution)/shard_map/forward/pallas_call | solution.py:216
  81.7 2.3 %collective-permute-start.1 = (bf16[328,1024]{1,0:T(8,128)(2,1)S(1)}, bf16[328,1024]{1,0:T(8,128)(2,1)S(1)}, u32[]{:S(2)}, u32[]{:S(2)}) collective-permute-start(bf16[328,1024]{1,0:T(8,128)(2,1)S(1)} %get-tuple-element.26), channel_id=1, source_target_pairs={{0,1},{1,0},{2,3},{3,2},{4,5},{5,4},{6,7},{7,6},{8,9},{9,8},{10,11... | collective-permute-start | bytes 2015240 | tf_op jit(solution)/shard_map/ppermute | solution.py:356
  84.0 0.8 shared_sum.1
  84.8 1.0 collective-permute-done.1.take_ref
  86.3 0.9 copy-done
  87.2 7.3 %all-to-all-start.1 = ((bf16[64,6,8,128]{3,2,1,0:T(8,128)(2,1)}), bf16[64,6,8,128]{3,2,1,0:T(8,128)(2,1)S(1)}, u32[]{:S(2)}, u32[]{:S(2)}) async-start(bf16[64,6,8,128]{3,2,1,0:T(8,128)(2,1)} %copy-done), calls=%async_computation.1 | async-start | bytes 1572864 | tf_op jit(solution)/shard_map/all_to_all | solution.py:373
  94.5 22.6 %all-to-all-done.1.recv_ref = bf16[64,6,8,128]{3,2,1,0:T(8,128)(2,1)S(1)} async-done(((bf16[64,6,8,128]{3,2,1,0:T(8,128)(2,1)}), bf16[64,6,8,128]{3,2,1,0:T(8,128)(2,1)S(1)}, u32[]{:S(2)}, u32[]{:S(2)}) %all-to-all-start.1) | async-done | bytes 786464 | tf_op jit(solution)/shard_map/all_to_all | solution.py:373
  117.0 1.8 %combine.1 = (bf16[8,136,128]{2,1,0:T(8,128)(2,1)S(1)}, f32[8,64]{1,0:T(8,128)S(1)}) custom-call(s32[2,128]{1,0:T(2,128)S(1)} %bitcast.11, s32[2,128]{1,0:T(2,128)S(1)} %get-tuple-element.23.rank_s.rank_ref, s32[1]{0:T(128)} %bitcast.3.me_s, bf16[64,6,8,128]{3,2,1,0:T(8,128)(2,1)S(1)} %all-to-all-done.1.recv_ref, s32[2,128]{1,0:T(2,128)S(1)} %bitcast.12, ...), custom_call_target="tpu_custom_call" | custom-call | tf_op jit(solution)/shard_map/combine/pallas_call | solution.py:317
  118.8 0.7 copy-done.8
  119.5 6.5 %all-to-all-start.2 = ((bf16[8,136,128]{2,1,0:T(8,128)(2,1)}), bf16[8,136,128]{2,1,0:T(8,128)(2,1)S(1)}, u32[]{:S(2)}, u32[]{:S(2)}) async-start(bf16[8,136,128]{2,1,0:T(8,128)(2,1)} %copy-done.8), calls=%async_computation.2 | async-start | bytes 557056 | tf_op jit(solution)/shard_map/all_to_all | solution.py:376
  126.0 1.0 copy-done.7
  127.0 1.9 %grads.1 = (bf16[1,128,2048]{2,1,0:T(8,128)(2,1)}, bf16[1,128,2048]{2,1,0:T(8,128)(2,1)}, bf16[1,128,2048]{2,1,0:T(8,128)(2,1)}, f32[3,128]{1,0:T(4,128)S(1)}) custom-call(s32[1]{0:T(128)} %bitcast.4.core_s, bf16[3,128,320]{2,1,0:T(8,128)(2,1)S(1)} %copy-done.7, bf16[2,320,1024]{2,1,0:T(8,128)(2,1)S(1)} %unpack.1.own_ref, ...), custom_call_target="tpu_custom_call" | custom-call | tf_op jit(solution)/shard_map/grads/pallas_call | solution.py:246
  129.9 5.7 %all-to-all-done.2.recv_ref = bf16[8,136,128]{2,1,0:T(8,128)(2,1)S(1)} async-done(((bf16[8,136,128]{2,1,0:T(8,128)(2,1)}), bf16[8,136,128]{2,1,0:T(8,128)(2,1)S(1)}, u32[]{:S(2)}, u32[]{:S(2)}) %all-to-all-start.2) | async-done | bytes 278560 | tf_op jit(solution)/shard_map/all_to_all | solution.py:376
  135.6 0.7 end.1
  (23 shorter events, 1.7 us)
Async XLA Ops:
  0.6 1.0 copy-start.4
  1.7 1.0 copy-start.5
  2.7 0.9 copy-start.9
  3.7 0.7 copy-start.10
  4.4 0.7 copy-start.12
  70.6 8.5 %copy-start.1 = (bf16[1,128,2048]{2,1,0:T(8,128)(2,1)S(1)}, bf16[1,128,2048]{2,1,0:T(8,128)(2,1)}, u32[]{:S(2)}) copy-start(bf16[1,128,2048]{2,1,0:T(8,128)(2,1)} %gate_ref.1) | copy-start | bytes 1572868
  70.6 8.5 %copy-start.2 = (bf16[1,128,2048]{2,1,0:T(8,128)(2,1)S(1)}, bf16[1,128,2048]{2,1,0:T(8,128)(2,1)}, u32[]{:S(2)}) copy-start(bf16[1,128,2048]{2,1,0:T(8,128)(2,1)} %up_ref.1) | copy-start | bytes 1572868
  70.6 8.5 %copy-start.3 = (bf16[1,128,2048]{2,1,0:T(8,128)(2,1)S(1)}, bf16[1,128,2048]{2,1,0:T(8,128)(2,1)}, u32[]{:S(2)}) copy-start(bf16[1,128,2048]{2,1,0:T(8,128)(2,1)} %down_ref.1) | copy-start | bytes 1572868
  71.3 7.7 %collective-permute-start = (bf16[2,320,1024]{2,1,0:T(8,128)(2,1)S(1)}, bf16[2,320,1024]{2,1,0:T(8,128)(2,1)S(1)}, u32[]{:S(2)}, u32[]{:S(2)}) collective-permute-start(bf16[2,320,1024]{2,1,0:T(8,128)(2,1)S(1)} %unpack.1.own_ref), channel_id=1, source_target_pairs={{0,1},{1,0},{2,3},{3,2},{4,5},{5,4},{6,7},{7,6},{8,9},{9,8},{10,11... | collective-permute-start | bytes 3932168 | tf_op jit(solution)/shard_map/ppermute | solution.py:356
  81.7 4.0 %copy-start.6 = (bf16[3,128,320]{2,1,0:T(8,128)(2,1)}, bf16[3,128,320]{2,1,0:T(8,128)(2,1)S(1)}, u32[]{:S(2)}) copy-start(bf16[3,128,320]{2,1,0:T(8,128)(2,1)S(1)} %get-tuple-element.31.delta_ref) | copy-start | bytes 737284
  81.7 4.0 %collective-permute-start.1 = (bf16[328,1024]{1,0:T(8,128)(2,1)S(1)}, bf16[328,1024]{1,0:T(8,128)(2,1)S(1)}, u32[]{:S(2)}, u32[]{:S(2)}) collective-permute-start(bf16[328,1024]{1,0:T(8,128)(2,1)S(1)} %get-tuple-element.26), channel_id=1, source_target_pairs={{0,1},{1,0},{2,3},{3,2},{4,5},{5,4},{6,7},{7,6},{8,9},{9,8},{10,11... | collective-permute-start | bytes 2015240 | tf_op jit(solution)/shard_map/ppermute | solution.py:356
  85.7 31.3 %copy-start.11 = (s32[128,2]{0,1:T(2,128)S(1)}, s32[128,2]{0,1:T(2,128)}, u32[]{:S(2)}) copy-start(s32[128,2]{0,1:T(2,128)} %param.10) | copy-start | bytes 3076
  86.3 0.9 copy-start
  87.2 29.8 %all-to-all-start.1 = ((bf16[64,6,8,128]{3,2,1,0:T(8,128)(2,1)}), bf16[64,6,8,128]{3,2,1,0:T(8,128)(2,1)S(1)}, u32[]{:S(2)}, u32[]{:S(2)}) async-start(bf16[64,6,8,128]{3,2,1,0:T(8,128)(2,1)} %copy-done), calls=%async_computation.1 | async-start | bytes 1572864 | tf_op jit(solution)/shard_map/all_to_all | solution.py:373
  118.8 0.7 copy-start.8
  119.5 16.1 %all-to-all-start.2 = ((bf16[8,136,128]{2,1,0:T(8,128)(2,1)}), bf16[8,136,128]{2,1,0:T(8,128)(2,1)S(1)}, u32[]{:S(2)}, u32[]{:S(2)}) async-start(bf16[8,136,128]{2,1,0:T(8,128)(2,1)} %copy-done.8), calls=%async_computation.2 | async-start | bytes 557056 | tf_op jit(solution)/shard_map/all_to_all | solution.py:376
  126.0 9.6 %copy-start.13 = (f32[128,2]{0,1:T(2,128)S(1)}, f32[128,2]{0,1:T(2,128)}, u32[]{:S(2)}) copy-start(f32[128,2]{0,1:T(2,128)} %param.11) | copy-start | bytes 3076
  126.0 1.0 copy-start.7

commit v2 on v1

v2 whole, which is shorter than its diff:
```python
import functools

import jax
import jax.numpy as jnp
from jax import lax
from jax.experimental import pallas as pl
from jax.experimental.pallas import tpu as pltpu
from jax.sharding import Mesh
from jax.sharding import PartitionSpec as P

EP = ("z", "y")
TP = ("x", "c")
BF, F32, I32 = jnp.bfloat16, jnp.float32, jnp.int32
LANES = 128
TILE = 8
HALF = TILE * LANES
SHARED = 2
GROUP = 16


def params(mib):
    return pltpu.CompilerParams(vmem_limit_bytes=mib * 1024 * 1024)


def in_vmem(n):
    return [pl.BlockSpec(memory_space=pltpu.VMEM)] * n


def in_smem(n):
    return [pl.BlockSpec(memory_space=pltpu.SMEM)] * n


def iota(shape, dim):
    return lax.broadcasted_iota(I32, shape, dim)


def ones_at(mask):
    return mask.astype(F32).astype(BF)


def dot(a, b, ca=1, cb=0):
    return lax.dot_general(a, b, (((ca,), (cb,)), ((), ())), preferred_element_type=F32)


def split2(v):
    hi = v.astype(BF).astype(F32)
    return hi, v - hi


def spread(ref, x):
    for j in range(TILE):
        cols = x[:, j * LANES : (j + 1) * LANES].astype(F32)
        ref[pl.ds(j, x.shape[0], stride=TILE), :] = cols


def gather_cols(ref, count, j):
    return ref[pl.ds(j, count, stride=TILE), :]


def send_kernel(
    cap, at_s, me_s, tok_ref, grad_ref, act_ref, ids_ref, w_ref, out_ref, rank_s,
    tok_v, grad_v, act_v, ids_s, w_s, seen_s, tok_t, grad_t, sems,
):
    del me_s
    count, width = grad_ref.shape
    experts = out_ref.shape[0]
    mine = pl.ds(pl.multiple_of((at_s[0] % 2) * HALF, HALF), HALF)
    line = pl.ds(pl.multiple_of((at_s[0] // 2) * LANES, LANES), LANES)
    pairs = (
        (act_ref.at[:, line], act_v),
        (grad_ref, grad_v),
        (tok_ref.at[:, mine], tok_v),
        (ids_ref, ids_s),
        (w_ref, w_s),
    )
    copies = [pltpu.make_async_copy(a, b, sems.at[i]) for i, (a, b) in enumerate(pairs)]
    for c in copies:
        c.start()
    for e in range(experts):
        seen_s[e] = 0
    out_ref[:, : 2 * cap] = jnp.zeros((experts, 2 * cap, TILE, LANES), BF)
    for c in copies:
        c.wait()
    spread(tok_t, tok_v[...])
    spread(grad_t, grad_v[:, mine])

    def one_token(t, carry):
        rows = pl.ds(pl.multiple_of(t * TILE, TILE), TILE)
        tok = tok_t[rows, :].astype(BF)
        grad = grad_t[rows, :]
        for k in range(2):
            e = ids_s[k, t]
            r = seen_s[e]
            seen_s[e] = r + 1
            rank_s[k, t] = r
            out_ref[e, r] = tok
            out_ref[e, cap + r] = (w_s[k, t] * grad).astype(BF)
        return carry

    lax.fori_loop(0, count, one_token, 0, unroll=8)

    half = LANES // 2
    act = act_v[...]
    swapped = jnp.concatenate([act[:, half:], act[:, :half]], axis=1)
    own = (at_s[0] % 2) * half
    keep = (iota(act.shape, 1) // half) * half == own
    twice = jnp.where(keep, act.astype(F32), swapped.astype(F32)).astype(BF)
    step = 2 * LANES
    block = width // experts
    for s in range(0, width, step):
        term = dot(grad_v[:, s : s + step], twice, 0, 0)
        term = term.reshape(step // block, 2, block // 2, LANES)
        lane = iota((step // block, block // 2, LANES), 2)
        both = jnp.where(lane < half, term[:, 0], term[:, 1]).astype(BF)
        out_ref[s // block : (s + step) // block, 2 * cap :] = both.reshape(
            step // block, SHARED, TILE, LANES
        )


def send_rows(at, me, tokens, out_grad, act, ids_t, w_t, cap, experts):
    count, width = out_grad.shape
    return pl.pallas_call(
        functools.partial(send_kernel, cap),
        in_specs=in_smem(2) + [pl.BlockSpec(memory_space=pltpu.HBM)] * 5,
        out_specs=in_vmem(1) + in_smem(1),
        out_shape=[
            jax.ShapeDtypeStruct((experts, 2 * cap + SHARED, TILE, LANES), BF),
            jax.ShapeDtypeStruct((2, count), I32),
        ],
        scratch_shapes=[
            pltpu.VMEM((count, HALF), BF),
            pltpu.VMEM((count, width), BF),
            pltpu.VMEM((count, LANES), BF),
            pltpu.SMEM((2, count), I32),
            pltpu.SMEM((2, count), F32),
            pltpu.SMEM((experts,), I32),
            pltpu.VMEM((count * TILE, LANES), F32),
            pltpu.VMEM((count * TILE, LANES), F32),
            pltpu.SemaphoreType.DMA((5,)),
        ],
        compiler_params=params(16),
        name="send_rows",
    )(at, me, tokens, out_grad, act, ids_t, w_t)


def shared_kernel(cap, recv_ref, out_ref, norm_ref):
    total = jnp.sum(recv_ref[:, 2 * cap :].astype(F32), axis=0).reshape(SHARED * TILE, LANES)
    half = LANES // 2
    out_ref[...] = jnp.concatenate([total[:, :half], total[:, half:]], axis=0)
    sq = jnp.sum(total * total, axis=0, keepdims=True)
    sq = sq + jnp.concatenate([sq[:, half:], sq[:, :half]], axis=1)
    norm_ref[...] = jnp.broadcast_to(sq, norm_ref.shape)


def shared_sum(recv, cap):
    return pl.pallas_call(
        functools.partial(shared_kernel, cap),
        in_specs=in_vmem(1),
        out_specs=in_vmem(2),
        out_shape=[
            jax.ShapeDtypeStruct((32, LANES // 2), F32),
            jax.ShapeDtypeStruct((TILE, LANES), F32),
        ],
        compiler_params=params(16),
        name="shared_sum",
    )(recv)


def unpack_kernel(cap, recv_ref, rows_ref, in_t, cot_t):
    n = recv_ref.shape[0]
    count = n * cap
    for k, ref in enumerate((in_t, cot_t)):
        tiles = recv_ref[:, k * cap : (k + 1) * cap].astype(F32)
        ref[...] = tiles.reshape(count * TILE, LANES)
        for j in range(TILE):
            cols = slice(j * LANES, (j + 1) * LANES)
            rows_ref[k, :, cols] = gather_cols(ref, count, j).astype(BF)


def unpack(recv, cap):
    count = recv.shape[0] * cap
    return pl.pallas_call(
        functools.partial(unpack_kernel, cap),
        in_specs=in_vmem(1),
        out_specs=pl.BlockSpec(memory_space=pltpu.VMEM),
        out_shape=jax.ShapeDtypeStruct((2, count, HALF), BF),
        scratch_shapes=[pltpu.VMEM((count * TILE, LANES), F32)] * 2,
        compiler_params=params(16),
        name="unpack",
    )(recv)


def products(side, rows_ref, gate_ref, up_ref, down_ref, sums):
    step = 2 * LANES
    for s in range(0, HALF, step):
        cols = pl.ds(pl.multiple_of(side * HALF + s, step), step)
        a, b = rows_ref[0, :, s : s + step], rows_ref[1, :, s : s + step]
        for k, (x, w) in enumerate(((a, gate_ref), (a, up_ref), (b, down_ref))):
            sums[k] = sums[k] + dot(x, w[0, :, cols], 1, 1)
    return sums


def half_kernel(core_s, own_ref, gate_ref, up_ref, down_ref, out_ref):
    sums = products(core_s[0], own_ref, gate_ref, up_ref, down_ref, [0.0] * 3)
    for k in range(3):
        out_ref[k] = sums[k]


def half_products(core, own, gate, up, down):
    return pl.pallas_call(
        half_kernel,
        in_specs=in_smem(1) + in_vmem(4),
        out_specs=pl.BlockSpec(memory_space=pltpu.VMEM),
        out_shape=jax.ShapeDtypeStruct((3, own.shape[1], gate.shape[1]), F32),
        compiler_params=params(16),
        name="half_products",
    )(core, own, gate, up, down)


def shares(side, deltas, gate_ref, up_ref, inner, ref):
    count = deltas.shape[0]
    for j in range(ref.shape[0]):
        cols = pl.ds(pl.multiple_of(j * 2 * LANES + side * LANES, LANES), LANES)
        w = jnp.concatenate([gate_ref[0, :, cols], up_ref[0, :, cols]], axis=0)
        ref[j, :count] = dot(deltas, w).astype(BF)
        ref[j, count:] = inner


def forward_kernel(
    cap, core_s, half_ref, other_ref, gate_ref, up_ref, down_ref, give_ref, delta_ref, inner_ref
):
    core = core_s[0]
    count = other_ref.shape[1]
    sums = products(1 - core, other_ref, gate_ref, up_ref, down_ref, [half_ref[k] for k in range(3)])
    gate_pre, up_pre, hidden_grad = sums
    sig = jax.nn.sigmoid(gate_pre)
    silu = gate_pre * sig
    hidden = (silu * up_pre).astype(BF)
    up_delta = (hidden_grad * silu).astype(BF)
    gate_delta = (hidden_grad * up_pre * sig * (1.0 + gate_pre * (1.0 - sig))).astype(BF)
    inner = jnp.sum(hidden.astype(F32) * hidden_grad, axis=1, keepdims=True)
    slot = iota((count, LANES), 0)
    lane = (slot // cap) % GROUP * TILE + slot % cap
    spots = jnp.where(lane == iota((count, LANES), 1), inner, 0.0)
    span = GROUP * cap
    lines = [jnp.sum(spots[s : s + span], axis=0, keepdims=True) for s in range(0, count, span)]
    tile = jnp.concatenate(split2(jnp.concatenate(lines, axis=0)), axis=0).astype(BF)
    inner_ref[...] = tile
    shares(1 - core, jnp.concatenate([gate_delta, up_delta], axis=1), gate_ref, up_ref, tile, give_ref)
    for k, d in enumerate((gate_delta, up_delta, hidden)):
        delta_ref[k] = d


def forward(core, half, other, gate, up, down, cap):
    count = other.shape[1]
    return pl.pallas_call(
        functools.partial(forward_kernel, cap),
        in_specs=in_smem(1) + in_vmem(5),
        out_specs=in_vmem(3),
        out_shape=[
            jax.ShapeDtypeStruct((TILE, count + TILE, LANES), BF),
            jax.ShapeDtypeStruct((3, count, gate.shape[1]), BF),
            jax.ShapeDtypeStruct((TILE, LANES), BF),
        ],
        compiler_params=params(24),
        name="forward",
    )(core, half, other, gate, up, down)


def keep_kernel(core_s, delta_ref, inner_ref, gate_ref, up_ref, keep_ref):
    deltas = jnp.concatenate([delta_ref[0], delta_ref[1]], axis=1)
    shares(core_s[0], deltas, gate_ref, up_ref, inner_ref[...], keep_ref)


def keep_shares(core, delta, inner, gate, up):
    return pl.pallas_call(
        keep_kernel,
        in_specs=in_smem(1) + in_vmem(4),
        out_specs=pl.BlockSpec(memory_space=pltpu.VMEM),
        out_shape=jax.ShapeDtypeStruct((TILE, delta.shape[1] + TILE, LANES), BF),
        compiler_params=params(16),
        name="keep_shares",
    )(core, delta, inner, gate, up)


def pair_kernel(a_ref, b_ref, out_ref):
    out_ref[...] = (a_ref[...].astype(F32) + b_ref[...].astype(F32)).astype(BF)


def pair_sum(a, b):
    return pl.pallas_call(
        pair_kernel,
        in_specs=in_vmem(2),
        out_specs=pl.BlockSpec(memory_space=pltpu.VMEM),
        out_shape=jax.ShapeDtypeStruct(a.shape, BF),
        compiler_params=params(16),
        name="pair_sum",
    )(a, b)


def grads_kernel(core_s, delta_ref, own_ref, other_ref, gate_ref, up_ref, down_ref, norm_ref):
    core = core_s[0]
    step = 2 * LANES
    for k, (out, which) in enumerate(((gate_ref, 0), (up_ref, 0), (down_ref, 1))):
        total = 0.0
        delta = delta_ref[k].astype(F32).T.astype(BF)
        for side, ref in ((core, own_ref), (1 - core, other_ref)):
            for s in range(0, HALF, step):
                g = dot(delta, ref[which, :, s : s + step])
                cols = pl.ds(pl.multiple_of(side * HALF + s, step), step)
                out[0, :, cols] = g.astype(BF)
                sq = g * g
                total = total + sq[:, :LANES] + sq[:, LANES:]
        norm_ref[k] = jnp.sum(total.T, axis=0, keepdims=True)


def grads(core, delta, own, other):
    feats = delta.shape[2]
    out = jax.ShapeDtypeStruct((1, feats, 2 * HALF), BF)
    return pl.pallas_call(
        grads_kernel,
        in_specs=in_smem(1) + in_vmem(3),
        out_specs=in_vmem(4),
        out_shape=[out, out, out, jax.ShapeDtypeStruct((3, 1, feats), F32)],
        compiler_params=params(24),
        name="grads",
    )(core, delta, own, other)


def back_kernel(cap, parts_ref, norm_ref, out_ref, sums, rows):
    n = out_ref.shape[0]
    count = n * cap
    total = parts_ref[0].astype(F32)
    for x in range(1, parts_ref.shape[0]):
        total = total + parts_ref[x].astype(F32)
    sums[...] = total
    for r in range(cap):
        rows[pl.ds(r, n, stride=TILE), :] = sums[pl.ds(r, n, stride=cap), :]
    lines = n // GROUP
    inner = split2(total[count : count + lines] + total[count + lines : count + 2 * lines])
    for r, part in zip((cap, cap + 2), inner):
        spread_lines = [
            jnp.broadcast_to(part[g : g + 1], (GROUP, LANES)) for g in range(lines)
        ]
        rows[pl.ds(r, n, stride=TILE), :] = jnp.concatenate(spread_lines, axis=0)
    norm_hi, norm_lo = split2(norm_ref[:1])
    norm = jnp.where(iota((1, LANES), 1) < LANES // 2, norm_hi, norm_lo)
    rows[pl.ds(cap + 1, n, stride=TILE), :] = jnp.broadcast_to(norm, (n, LANES))
    out_ref[...] = rows[...].astype(BF).reshape(n, TILE, LANES)


def back_rows(parts, norms, n, cap):
    return pl.pallas_call(
        functools.partial(back_kernel, cap),
        in_specs=in_vmem(2),
        out_specs=pl.BlockSpec(memory_space=pltpu.VMEM),
        out_shape=jax.ShapeDtypeStruct((n, TILE, LANES), BF),
        scratch_shapes=[
            pltpu.VMEM(parts.shape[1:], F32),
            pltpu.VMEM((n * TILE, LANES), F32),
        ],
        compiler_params=params(16),
        name="back_rows",
    )(parts, norms)


def end_kernel(cap, me_s, recv_ref, ids_ref, rank_ref, w_ref, tok_ref, route_ref, norm_ref):
    n = recv_ref.shape[0]
    count = ids_ref.shape[1]
    rows = recv_ref[...].reshape(n * TILE, LANES)
    o = iota((n * TILE, count), 0)
    first = [ids_ref[k : k + 1, :] * TILE for k in range(2)]
    rank = [rank_ref[k : k + 1, :] for k in range(2)]
    pick = ones_at((o == first[0] + rank[0]) | (o == first[1] + rank[1]))
    tok_ref[...] = dot(pick, rows, 0, 0).astype(BF)
    route = []
    for k in range(2):
        pick = ones_at((o == first[k] + cap) | (o == first[k] + cap + 2))
        got = dot(rows, pick, 0, 0)
        use = iota((LANES, count), 0) == (me_s[0] % GROUP) * TILE + rank[k]
        route.append(jnp.sum(jnp.where(use, got, 0.0), axis=0, keepdims=True))
    route_ref[...] = jnp.concatenate(route, axis=0) / w_ref[...]
    sums = dot(ones_at(iota((TILE, n * TILE), 1) % TILE == cap + 1), rows)
    norm_ref[...] = sums[:1, : LANES // 2] + sums[:1, LANES // 2 :]


def end(me, recv, ids_t, rank, w_t, cap):
    count = ids_t.shape[1]
    return pl.pallas_call(
        functools.partial(end_kernel, cap),
        in_specs=in_smem(1) + in_vmem(4),
        out_specs=in_vmem(3),
        out_shape=[
            jax.ShapeDtypeStruct((count, LANES), BF),
            jax.ShapeDtypeStruct((2, count), F32),
            jax.ShapeDtypeStruct((1, LANES // 2), F32),
        ],
        compiler_params=params(16),
        name="end",
    )(me, recv, ids_t, rank, w_t)


def swap(v):
    return lax.ppermute(v, "c", [(0, 1), (1, 0)])


def local(tokens, out_grad, expert_ids, route_weights, gate_proj, up_proj, down_proj, shared_act):
    n = lax.axis_size(EP)
    cap = 5 * tokens.shape[0] * expert_ids.shape[1] // (4 * n)
    core = lax.axis_index("c").reshape(1)
    at = lax.axis_index(TP).reshape(1)
    me = lax.axis_index(EP).reshape(1)
    ids_t, w_t = expert_ids.T, route_weights.T
    here = (tokens, out_grad, shared_act, ids_t, w_t)
    here = [pltpu.with_memory_space_constraint(v, pltpu.HBM) for v in here]
    sent, rank = send_rows(at, me, *here, cap, n)
    recv = lax.all_to_all(sent, EP, 0, 0, tiled=True)
    own = unpack(recv, cap)
    other = swap(own)
    half = half_products(core, own, gate_proj, up_proj, down_proj)
    shared, norms = shared_sum(recv, cap)
    give, delta, inner = forward(core, half, other, gate_proj, up_proj, down_proj, cap)
    take = swap(give)
    keep = keep_shares(core, delta, inner, gate_proj, up_proj)
    parts = lax.all_to_all(pair_sum(keep, take), "x", 0, 0, tiled=True)
    gate_grad, up_grad, down_grad, row_norms = grads(core, delta, own, other)
    back = back_rows(parts, norms, n, cap)
    returned = lax.all_to_all(back, EP, 0, 0, tiled=True)
    token_grad, route_grad, shared_norms = end(me, returned, ids_t, rank, w_t, cap)
    return (
        token_grad,
        route_grad.T,
        gate_grad,
        up_grad,
        down_grad,
        row_norms.transpose(1, 0, 2),
        shared.T,
        shared_norms.reshape(-1),
    )


def solution(mesh):
    torus = Mesh(mesh.devices.reshape(8, 8, mesh.shape["tp"] // 2, 2), (*EP, *TP))
    return jax.shard_map(
        local,
        mesh=torus,
        in_specs=(
            P(EP, None),
            P(EP, None),
            P(EP, None),
            P(EP, None),
            P(EP, TP, None),
            P(EP, TP, None),
            P(EP, TP, None),
            P(EP, None),
        ),
        out_specs=(
            P(EP, TP),
            P(EP, None),
            P(EP, TP, None),
            P(EP, TP, None),
            P(EP, TP, None),
            P(EP, None, TP),
            P(TP, EP),
            P(TP),
        ),
        check_vma=False,
    )
```

time: 139 us -> 131 us (0.942); the launches traced: 136 us -> 131 us
  local copies, waits for them, and re-layouts: 8.02 us -> 4.43 us
  waiting for transfers between devices: 31.9 us -> 30.3 us
    all_to_all x1, waiting for transfers between devices: 22.6 us -> 7.41 us  [local(): returned = lax.all_to_all(back, EP, 0, 0, tiled=True)]
    all_to_all x1, waiting for transfers between devices: 5.71 us -> 19.8 us  [local(): parts = lax.all_to_all(pair_sum(keep, take), 'x', 0, 0, tiled=True)]
    unnamed x29 -> x28, local copies, waits for them, and re-layouts: 7.51 us -> 4.43 us
    pallas_call x5 -> x7, Pallas kernels: 8.35 us -> 7.93 us  [the longest x1 3.37 us: send_rows(): pl.pallas_call(functools.partial(send_kernel, cap), in_specs=in_smem(2) +...]
  transfers between devices with their start and end apart: 4 -> 4, of which waited for: 4 -> 4; matrix products, arithmetic and copies ran while one was open for 1% -> 0% of each run, Pallas kernels for 2% -> 3%
where the time goes in v2:
time: 131 us
  blocking collectives  62.8 us (48%)
  waiting for transfers between devices  30.3 us (23%)
  starting transfers between devices  21.2 us (16%)
  Pallas kernels  11.3 us (9%)
  local copies, waits for them, and re-layouts  4.43 us (3%)
    all_to_all x1, blocking collectives, local(): recv = lax.all_to_all(sent, EP, 0, 0, tiled=True)  62.8 us
    all_to_all x1, waiting for transfers between devices, local(): parts = lax.all_to_all(pair_sum(keep, take), 'x', 0, 0, tiled=True)  19.8 us
    all_to_all x1, waiting for transfers between devices, local(): returned = lax.all_to_all(back, EP, 0, 0, tiled=True)  7.41 us
    all_to_all x1, starting transfers between devices, local(): returned = lax.all_to_all(back, EP, 0, 0, tiled=True)  7.38 us
    ppermute x2, starting transfers between devices, swap(): return lax.ppermute(v, 'c', [(0, 1), (1, 0)])  7.38 us
    all_to_all x1, starting transfers between devices, local(): parts = lax.all_to_all(pair_sum(keep, take), 'x', 0, 0, tiled=True)  6.49 us
    unnamed x28, local copies, waits for them, and re-layouts  4.43 us
    pallas_call x1, Pallas kernels, send_rows(): pl.pallas_call(functools.partial(send_kernel, cap), in_specs=in_smem(2) +...  3.37 us
  transfers between devices with their start and end apart: 4, of which 4 were waited for; matrix products, arithmetic and copies ran while one was open for 0% of the time, Pallas kernels for 3%

profile of v2, /device:TPU:1, one launch (start us, length us, event | category | flops | bytes accessed | tf_op | source)
XLA Modules:
  0.0 130.9 jit_solution(4447399307181506514)
XLA Ops:
  0.6 3.4 %send_rows.1 = (bf16[64,12,8,128]{3,2,1,0:T(8,128)(2,1)S(1)}, s32[2,128]{1,0:T(2,128)S(1)}) custom-call(s32[1]{0:T(128)} %bitcast.2.at_s, s32[1]{0:T(128)} %bitcast.me_s, bf16[128,2048]{1,0:T(8,128)(2,1)} %tok_ref.1, bf16[128,2048]{1,0:T(8,128)(2,1)} %grad_ref.1, bf16[128,1024]{1,0:T(8,128)(2,1)} %act_ref.1, s32[2,128]{1,0:T(2,128)} %bitcast.9, ...), custom_call_target="tpu_custom_call" | custom-call | tf_op jit(solution)/shard_map/send_rows/pallas_call | solution.py:122
  4.0 62.8 %all_to_all.15.recv_ref = bf16[64,12,8,128]{3,2,1,0:T(8,128)(2,1)S(1)} all-to-all(bf16[64,12,8,128]{3,2,1,0:T(8,128)(2,1)S(1)} %get-tuple-element.22), channel_id=1, replica_groups=mesh['z'=8,'y'=8,'x'=8,'c'=2] {'z','y'}, dimensions={0} | all-to-all | bytes 3145728 | tf_op jit(solution)/shard_map/all_to_all | solution.py:417
  66.9 0.7 unpack.1.own_ref
  67.6 5.1 %collective-permute-start = (bf16[2,320,1024]{2,1,0:T(8,128)(2,1)S(1)}, bf16[2,320,1024]{2,1,0:T(8,128)(2,1)S(1)}, u32[]{:S(2)}, u32[]{:S(2)}) collective-permute-start(bf16[2,320,1024]{2,1,0:T(8,128)(2,1)S(1)} %unpack.1.own_ref), channel_id=1, source_target_pairs={{0,1},{1,0},{2,3},{3,2},{4,5},{5,4},{6,7},{7,6},{8,9},{9,8},{10,11... | collective-permute-start | bytes 3932168 | tf_op jit(solution)/shard_map/ppermute | solution.py:404
  72.7 0.7 half_products.1.half_ref
  73.4 1.9 %collective-permute-done.other_ref = bf16[2,320,1024]{2,1,0:T(8,128)(2,1)S(1)} collective-permute-done((bf16[2,320,1024]{2,1,0:T(8,128)(2,1)S(1)}, bf16[2,320,1024]{2,1,0:T(8,128)(2,1)S(1)}, u32[]{:S(2)}, u32[]{:S(2)}) %collective-permute-start) | collective-permute-done | bytes 1310752 | tf_op jit(solution)/shard_map/ppermute | solution.py:404
  75.3 1.5 %forward.1 = (bf16[8,328,128]{2,1,0:T(8,128)(2,1)S(1)}, bf16[3,320,128]{2,1,0:T(8,128)(2,1)S(1)}, bf16[8,128]{1,0:T(8,128)(2,1)S(1)}) custom-call(s32[1]{0:T(128)} %bitcast.1.core_s, f32[3,320,128]{2,1,0:T(8,128)S(1)} %half_products.1.half_ref, bf16[2,320,1024]{2,1,0:T(8,128)(2,1)S(1)} %collective-permute-done.other_ref, ...), custom_call_target="tpu_custom_call" | custom-call | tf_op jit(solution)/shard_map/forward/pallas_call | solution.py:256
  76.8 2.3 %collective-permute-start.1 = (bf16[8,328,128]{2,1,0:T(8,128)(2,1)S(1)}, bf16[8,328,128]{2,1,0:T(8,128)(2,1)S(1)}, u32[]{:S(2)}, u32[]{:S(2)}) collective-permute-start(bf16[8,328,128]{2,1,0:T(8,128)(2,1)S(1)} %get-tuple-element.25), channel_id=1, source_target_pairs={{0,1},{1,0},{2,3},{3,2},{4,5},{5,4},{6,7},{7,6},{8,9},{9,8},{10,11... | collective-permute-start | bytes 2015240 | tf_op jit(solution)/shard_map/ppermute | solution.py:404
  79.1 0.5 keep_shares.1.a_ref
  79.7 1.2 collective-permute-done.1.b_ref
  80.9 0.2 pair_sum.1
  81.0 0.9 copy-done.4
  81.9 6.5 %all-to-all-start.1 = ((bf16[8,328,128]{2,1,0:T(8,128)(2,1)}), bf16[8,328,128]{2,1,0:T(8,128)(2,1)S(1)}, u32[]{:S(2)}, u32[]{:S(2)}) async-start(bf16[8,328,128]{2,1,0:T(8,128)(2,1)} %copy-done.4), calls=%async_computation.1 | async-start | bytes 1343488 | tf_op jit(solution)/shard_map/all_to_all | solution.py:425
  88.4 0.8 shared_sum.1
  89.1 0.6 copy-done.8
  89.7 19.8 %all-to-all-done.1.parts_ref = bf16[8,328,128]{2,1,0:T(8,128)(2,1)S(1)} async-done(((bf16[8,328,128]{2,1,0:T(8,128)(2,1)}), bf16[8,328,128]{2,1,0:T(8,128)(2,1)S(1)}, u32[]{:S(2)}, u32[]{:S(2)}) %all-to-all-start.1) | async-done | bytes 671776 | tf_op jit(solution)/shard_map/all_to_all | solution.py:425
  109.5 0.7 copy-done.9
  110.2 0.8 back_rows.1
  111.0 7.4 %all-to-all-start.2 = ((bf16[64,8,128]{2,1,0:T(8,128)(2,1)}), bf16[64,8,128]{2,1,0:T(8,128)(2,1)S(1)}, u32[]{:S(2)}, u32[]{:S(2)}) async-start(bf16[64,8,128]{2,1,0:T(8,128)(2,1)} %back_rows.1), calls=%async_computation.2 | async-start | bytes 262144 | tf_op jit(solution)/shard_map/all_to_all | solution.py:428
  118.4 1.3 copy-done.1
  119.7 0.9 copy-done.7
  120.7 1.9 %grads.1 = (bf16[1,128,2048]{2,1,0:T(8,128)(2,1)}, bf16[1,128,2048]{2,1,0:T(8,128)(2,1)}, bf16[1,128,2048]{2,1,0:T(8,128)(2,1)}, f32[3,1,128]{2,1,0:T(1,128)}) custom-call(s32[1]{0:T(128)} %bitcast.1.core_s, bf16[3,320,128]{2,1,0:T(8,128)(2,1)S(1)} %copy-done.7, bf16[2,320,1024]{2,1,0:T(8,128)(2,1)S(1)} %unpack.1.own_ref, bf16[2,320,1024]{2,1,0:T(8,128)(2,1)S(1)} %copy-done.1), custom_call_target="tpu_custom_call" | custom-call | tf_op jit(solution)/shard_map/grads/pallas_call | solution.py:320
  122.5 7.4 %all-to-all-done.2.recv_ref = bf16[64,8,128]{2,1,0:T(8,128)(2,1)S(1)} async-done(((bf16[64,8,128]{2,1,0:T(8,128)(2,1)}), bf16[64,8,128]{2,1,0:T(8,128)(2,1)S(1)}, u32[]{:S(2)}, u32[]{:S(2)}) %all-to-all-start.2) | async-done | bytes 131104 | tf_op jit(solution)/shard_map/all_to_all | solution.py:428
  129.9 0.9 end.1
  (23 shorter events, 0.0 us)
Async XLA Ops:
  4.0 62.8 %copy-start.12 = (s32[2,128]{1,0:T(2,128)}, s32[2,128]{1,0:T(2,128)S(1)}, u32[]{:S(2)}) copy-start(s32[2,128]{1,0:T(2,128)S(1)} %get-tuple-element.27.rank_ref) | copy-start | bytes 3076
  66.9 5.8 %copy-start.2 = (bf16[1,128,2048]{2,1,0:T(8,128)(2,1)S(1)}, bf16[1,128,2048]{2,1,0:T(8,128)(2,1)}, u32[]{:S(2)}) copy-start(bf16[1,128,2048]{2,1,0:T(8,128)(2,1)} %gate_ref.5) | copy-start | bytes 1572868
  66.9 5.8 %copy-start.3 = (bf16[1,128,2048]{2,1,0:T(8,128)(2,1)S(1)}, bf16[1,128,2048]{2,1,0:T(8,128)(2,1)}, u32[]{:S(2)}) copy-start(bf16[1,128,2048]{2,1,0:T(8,128)(2,1)} %up_ref.5) | copy-start | bytes 1572868
  66.9 5.8 %copy-start.5 = (bf16[1,128,2048]{2,1,0:T(8,128)(2,1)S(1)}, bf16[1,128,2048]{2,1,0:T(8,128)(2,1)}, u32[]{:S(2)}) copy-start(bf16[1,128,2048]{2,1,0:T(8,128)(2,1)} %down_ref.3) | copy-start | bytes 1572868
  67.6 7.7 %collective-permute-start = (bf16[2,320,1024]{2,1,0:T(8,128)(2,1)S(1)}, bf16[2,320,1024]{2,1,0:T(8,128)(2,1)S(1)}, u32[]{:S(2)}, u32[]{:S(2)}) collective-permute-start(bf16[2,320,1024]{2,1,0:T(8,128)(2,1)S(1)} %unpack.1.own_ref), channel_id=1, source_target_pairs={{0,1},{1,0},{2,3},{3,2},{4,5},{5,4},{6,7},{7,6},{8,9},{9,8},{10,11... | collective-permute-start | bytes 3932168 | tf_op jit(solution)/shard_map/ppermute | solution.py:404
  75.3 1.5 %copy-start = (bf16[2,320,1024]{2,1,0:T(8,128)(2,1)}, bf16[2,320,1024]{2,1,0:T(8,128)(2,1)S(1)}, u32[]{:S(2)}) copy-start(bf16[2,320,1024]{2,1,0:T(8,128)(2,1)S(1)} %collective-permute-done.other_ref) | copy-start | bytes 3932164
  76.8 2.8 %copy-start.6 = (bf16[3,320,128]{2,1,0:T(8,128)(2,1)}, bf16[3,320,128]{2,1,0:T(8,128)(2,1)S(1)}, u32[]{:S(2)}) copy-start(bf16[3,320,128]{2,1,0:T(8,128)(2,1)S(1)} %get-tuple-element.23.delta_ref) | copy-start | bytes 737284
  76.8 4.0 %collective-permute-start.1 = (bf16[8,328,128]{2,1,0:T(8,128)(2,1)S(1)}, bf16[8,328,128]{2,1,0:T(8,128)(2,1)S(1)}, u32[]{:S(2)}, u32[]{:S(2)}) collective-permute-start(bf16[8,328,128]{2,1,0:T(8,128)(2,1)S(1)} %get-tuple-element.25), channel_id=1, source_target_pairs={{0,1},{1,0},{2,3},{3,2},{4,5},{5,4},{6,7},{7,6},{8,9},{9,8},{10,11... | collective-permute-start | bytes 2015240 | tf_op jit(solution)/shard_map/ppermute | solution.py:404
  81.0 0.9 copy-start.4
  81.9 27.6 %all-to-all-start.1 = ((bf16[8,328,128]{2,1,0:T(8,128)(2,1)}), bf16[8,328,128]{2,1,0:T(8,128)(2,1)S(1)}, u32[]{:S(2)}, u32[]{:S(2)}) async-start(bf16[8,328,128]{2,1,0:T(8,128)(2,1)} %copy-done.4), calls=%async_computation.1 | async-start | bytes 1343488 | tf_op jit(solution)/shard_map/all_to_all | solution.py:425
  89.1 0.6 copy-start.8
  109.5 0.7 copy-start.9
  111.0 18.9 %copy-start.10 = (s32[128,2]{0,1:T(2,128)S(1)}, s32[128,2]{0,1:T(2,128)}, u32[]{:S(2)}) copy-start(s32[128,2]{0,1:T(2,128)} %param.10) | copy-start | bytes 3076
  111.0 18.9 %copy-start.11 = (f32[128,2]{0,1:T(2,128)S(1)}, f32[128,2]{0,1:T(2,128)}, u32[]{:S(2)}) copy-start(f32[128,2]{0,1:T(2,128)} %param.11) | copy-start | bytes 3076
  111.0 18.9 %copy-start.13 = (s32[2,128]{1,0:T(2,128)S(1)}, s32[2,128]{1,0:T(2,128)}, u32[]{:S(2)}) copy-start(s32[2,128]{1,0:T(2,128)} %copy-done.12) | copy-start | bytes 3076
  111.0 18.9 %all-to-all-start.2 = ((bf16[64,8,128]{2,1,0:T(8,128)(2,1)}), bf16[64,8,128]{2,1,0:T(8,128)(2,1)S(1)}, u32[]{:S(2)}, u32[]{:S(2)}) async-start(bf16[64,8,128]{2,1,0:T(8,128)(2,1)} %back_rows.1), calls=%async_computation.2 | async-start | bytes 262144 | tf_op jit(solution)/shard_map/all_to_all | solution.py:428
  118.4 1.3 %copy-start.1 = (bf16[2,320,1024]{2,1,0:T(8,128)(2,1)S(1)}, bf16[2,320,1024]{2,1,0:T(8,128)(2,1)}, u32[]{:S(2)}) copy-start(bf16[2,320,1024]{2,1,0:T(8,128)(2,1)} %copy-done) | copy-start | bytes 3932164
  119.7 0.9 copy-start.7

commit v3 on v2

--- a/solution.py
+++ b/solution.py
@@ -283,19 +283,44 @@
     )(core, delta, inner, gate, up)
 
 
-def pair_kernel(a_ref, b_ref, out_ref):
-    out_ref[...] = (a_ref[...].astype(F32) + b_ref[...].astype(F32)).astype(BF)
-
-
-def pair_sum(a, b):
-    return pl.pallas_call(
-        pair_kernel,
-        in_specs=in_vmem(2),
+def back_kernel(cap, keep_ref, take_ref, norm_ref, out_ref, sums, rows):
+    n_x = keep_ref.shape[0]
+    n = out_ref.shape[0] // n_x
+    count = n * cap
+    lines = n // GROUP
+    step = n_x * TILE
+    last = keep_ref[0, count:].astype(F32) + take_ref[0, count:].astype(F32)
+    hi, lo = split2(last[:lines] + last[lines:])
+    norm_hi, norm_lo = split2(norm_ref[:1])
+    norm = jnp.where(iota((1, LANES), 1) < LANES // 2, norm_hi, norm_lo)
+    extra = [
+        jnp.concatenate([jnp.broadcast_to(v[g : g + 1], (GROUP, LANES)) for g in range(lines)], axis=0)
+        for v in (hi, lo)
+    ]
+    extra.insert(1, jnp.broadcast_to(norm, (n, LANES)))
+    for x in range(n_x):
+        sums[x] = keep_ref[x, :count].astype(F32) + take_ref[x, :count].astype(F32)
+        for r in range(cap):
+            rows[pl.ds(x * TILE + r, n, stride=step), :] = sums[x, pl.ds(r, n, stride=cap), :]
+        for r, v in enumerate(extra):
+            rows[pl.ds(x * TILE + cap + r, n, stride=step), :] = v
+    out_ref[...] = rows[...].astype(BF).reshape(out_ref.shape)
+
+
+def back_rows(keep, take, norms, n, cap):
+    n_x = keep.shape[0]
+    return pl.pallas_call(
+        functools.partial(back_kernel, cap),
+        in_specs=in_vmem(3),
         out_specs=pl.BlockSpec(memory_space=pltpu.VMEM),
-        out_shape=jax.ShapeDtypeStruct(a.shape, BF),
-        compiler_params=params(16),
-        name="pair_sum",
-    )(a, b)
+        out_shape=jax.ShapeDtypeStruct((n * n_x, TILE, LANES), BF),
+        scratch_shapes=[
+            pltpu.VMEM((n_x, n * cap, LANES), F32),
+            pltpu.VMEM((n * n_x * TILE, LANES), F32),
+        ],
+        compiler_params=params(24),
+        name="back_rows",
+    )(keep, take, norms)
 
 
 def grads_kernel(core_s, delta_ref, own_ref, other_ref, gate_ref, up_ref, down_ref, norm_ref):
@@ -327,48 +352,18 @@
     )(core, delta, own, other)
 
 
-def back_kernel(cap, parts_ref, norm_ref, out_ref, sums, rows):
-    n = out_ref.shape[0]
-    count = n * cap
-    total = parts_ref[0].astype(F32)
-    for x in range(1, parts_ref.shape[0]):
-        total = total + parts_ref[x].astype(F32)
-    sums[...] = total
-    for r in range(cap):
-        rows[pl.ds(r, n, stride=TILE), :] = sums[pl.ds(r, n, stride=cap), :]
-    lines = n // GROUP
-    inner = split2(total[count : count + lines] + total[count + lines : count + 2 * lines])
-    for r, part in zip((cap, cap + 2), inner):
-        spread_lines = [
-            jnp.broadcast_to(part[g : g + 1], (GROUP, LANES)) for g in range(lines)
-        ]
-        rows[pl.ds(r, n, stride=TILE), :] = jnp.concatenate(spread_lines, axis=0)
-    norm_hi, norm_lo = split2(norm_ref[:1])
-    norm = jnp.where(iota((1, LANES), 1) < LANES // 2, norm_hi, norm_lo)
-    rows[pl.ds(cap + 1, n, stride=TILE), :] = jnp.broadcast_to(norm, (n, LANES))
-    out_ref[...] = rows[...].astype(BF).reshape(n, TILE, LANES)
-
-
-def back_rows(parts, norms, n, cap):
-    return pl.pallas_call(
-        functools.partial(back_kernel, cap),
-        in_specs=in_vmem(2),
-        out_specs=pl.BlockSpec(memory_space=pltpu.VMEM),
-        out_shape=jax.ShapeDtypeStruct((n, TILE, LANES), BF),
-        scratch_shapes=[
-            pltpu.VMEM(parts.shape[1:], F32),
-            pltpu.VMEM((n * TILE, LANES), F32),
-        ],
-        compiler_params=params(16),
-        name="back_rows",
-    )(parts, norms)
-
-
-def end_kernel(cap, me_s, recv_ref, ids_ref, rank_ref, w_ref, tok_ref, route_ref, norm_ref):
-    n = recv_ref.shape[0]
+def end_kernel(cap, n_x, at_s, me_s, recv_ref, ids_ref, rank_ref, w_ref, tok_ref, route_ref, norm_ref):
+    n = recv_ref.shape[0] // n_x
     count = ids_ref.shape[1]
-    rows = recv_ref[...].reshape(n * TILE, LANES)
-    o = iota((n * TILE, count), 0)
+    parts = recv_ref[...].reshape(n, n_x, TILE, LANES)
+    norm_row = iota((n, TILE, LANES), 1) == cap + 1
+    total = jnp.zeros((n, TILE, LANES), F32)
+    for x in range(n_x):
+        part = parts[:, x].astype(F32)
+        total = total + jnp.where(norm_row & (at_s[0] // 2 != x), 0.0, part)
+    hi, lo = split2(total.reshape(n * TILE, LANES))
+    rows = jnp.concatenate([hi, lo], axis=0).astype(BF)
+    o = iota((2 * n * TILE, count), 0) % (n * TILE)
     first = [ids_ref[k : k + 1, :] * TILE for k in range(2)]
     rank = [rank_ref[k : k + 1, :] for k in range(2)]
     pick = ones_at((o == first[0] + rank[0]) | (o == first[1] + rank[1]))
@@ -380,15 +375,15 @@
         use = iota((LANES, count), 0) == (me_s[0] % GROUP) * TILE + rank[k]
         route.append(jnp.sum(jnp.where(use, got, 0.0), axis=0, keepdims=True))
     route_ref[...] = jnp.concatenate(route, axis=0) / w_ref[...]
-    sums = dot(ones_at(iota((TILE, n * TILE), 1) % TILE == cap + 1), rows)
+    sums = dot(ones_at(iota((TILE, 2 * n * TILE), 1) % TILE == cap + 1), rows)
     norm_ref[...] = sums[:1, : LANES // 2] + sums[:1, LANES // 2 :]
 
 
-def end(me, recv, ids_t, rank, w_t, cap):
+def end(at, me, recv, ids_t, rank, w_t, cap, n_x):
     count = ids_t.shape[1]
     return pl.pallas_call(
-        functools.partial(end_kernel, cap),
-        in_specs=in_smem(1) + in_vmem(4),
+        functools.partial(end_kernel, cap, n_x),
+        in_specs=in_smem(2) + in_vmem(4),
         out_specs=in_vmem(3),
         out_shape=[
             jax.ShapeDtypeStruct((count, LANES), BF),
@@ -397,7 +392,7 @@
         ],
         compiler_params=params(16),
         name="end",
-    )(me, recv, ids_t, rank, w_t)
+    )(at, me, recv, ids_t, rank, w_t)
 
 
 def swap(v):
@@ -422,11 +417,12 @@
     give, delta, inner = forward(core, half, other, gate_proj, up_proj, down_proj, cap)
     take = swap(give)
     keep = keep_shares(core, delta, inner, gate_proj, up_proj)
-    parts = lax.all_to_all(pair_sum(keep, take), "x", 0, 0, tiled=True)
+    back = back_rows(keep, take, norms, n, cap)
+    returned = lax.all_to_all(back, (*EP, "x"), 0, 0, tiled=True)
     gate_grad, up_grad, down_grad, row_norms = grads(core, delta, own, other)
-    back = back_rows(parts, norms, n, cap)
-    returned = lax.all_to_all(back, EP, 0, 0, tiled=True)
-    token_grad, route_grad, shared_norms = end(me, returned, ids_t, rank, w_t, cap)
+    token_grad, route_grad, shared_norms = end(
+        at, me, returned, ids_t, rank, w_t, cap, lax.axis_size("x")
+    )
     return (
         token_grad,
         route_grad.T,

time: 131 us -> 137 us (1.046)
  starting transfers between devices: 21.2 us -> 30 us
  local copies, waits for them, and re-layouts: 4.43 us -> 1.01 us
  Pallas kernels: 11.3 us -> 13.9 us
  waiting for transfers between devices: 30.3 us -> 28.3 us
    all_to_all x2 -> x1, starting transfers between devices: 13.9 us -> 22.6 us  [local(): returned = lax.all_to_all(back, (*EP, 'x'), 0, 0, tiled=True)]
    unnamed x28 -> x12, local copies, waits for them, and re-layouts: 4.43 us -> 1.01 us
    pallas_call x3 -> x2, Pallas kernels: 1.89 us -> 4.48 us  [the longest x1 2.53 us: end(): pl.pallas_call(functools.partial(end_kernel, cap, n_x), in_specs=in_smem(...]
    all_to_all x2 -> x1, waiting for transfers between devices: 27.2 us -> 25.9 us  [local(): returned = lax.all_to_all(back, (*EP, 'x'), 0, 0, tiled=True)]
  transfers between devices with their start and end apart: 4 -> 3, of which waited for: 4 -> 3; matrix products, arithmetic and copies ran while one was open for 0% -> 0% of each run, Pallas kernels for 3% -> 3%
where the time goes in v3:
time: 137 us
  blocking collectives  62.8 us (46%)
  starting transfers between devices  30 us (22%)
  waiting for transfers between devices  28.3 us (21%)
  Pallas kernels  13.9 us (10%)
    all_to_all x1, blocking collectives, local(): recv = lax.all_to_all(sent, EP, 0, 0, tiled=True)  62.8 us
    all_to_all x1, waiting for transfers between devices, local(): returned = lax.all_to_all(back, (*EP, 'x'), 0, 0, tiled=True)  25.9 us
    all_to_all x1, starting transfers between devices, local(): returned = lax.all_to_all(back, (*EP, 'x'), 0, 0, tiled=True)  22.6 us
    ppermute x2, starting transfers between devices, swap(): return lax.ppermute(v, 'c', [(0, 1), (1, 0)])  7.35 us
    pallas_call x1, Pallas kernels, send_rows(): pl.pallas_call(functools.partial(send_kernel, cap), in_specs=in_smem(2) +...  3.37 us
  transfers between devices with their start and end apart: 3, of which 3 were waited for; matrix products, arithmetic and copies ran while one was open for 0% of the time, Pallas kernels for 3%

profile of v3, /device:TPU:1, one launch (start us, length us, event | category | flops | bytes accessed | tf_op | source)
XLA Modules:
  0.0 136.7 jit_solution(3981885790414533705)
XLA Ops:
  0.6 3.4 %send_rows.1 = (bf16[64,12,8,128]{3,2,1,0:T(8,128)(2,1)S(1)}, s32[2,128]{1,0:T(2,128)S(1)}) custom-call(s32[1]{0:T(128)} %bitcast.at_s, s32[1]{0:T(128)} %bitcast.1.me_s, bf16[128,2048]{1,0:T(8,128)(2,1)} %tok_ref.1, bf16[128,2048]{1,0:T(8,128)(2,1)} %grad_ref.1, bf16[128,1024]{1,0:T(8,128)(2,1)} %act_ref.1, s32[2,128]{1,0:T(2,128)} %bitcast.9, ...), custom_call_target="tpu_custom_call" | custom-call | tf_op jit(solution)/shard_map/send_rows/pallas_call | solution.py:122
  4.0 62.8 %all_to_all.10.recv_ref = bf16[64,12,8,128]{3,2,1,0:T(8,128)(2,1)S(1)} all-to-all(bf16[64,12,8,128]{3,2,1,0:T(8,128)(2,1)S(1)} %get-tuple-element.22), channel_id=1, replica_groups=mesh['z'=8,'y'=8,'x'=8,'c'=2] {'z','y'}, dimensions={0} | all-to-all | bytes 3145728 | tf_op jit(solution)/shard_map/all_to_all | solution.py:412
  66.9 0.7 unpack.1.own_ref
  67.6 5.1 %collective-permute-start = (bf16[2,320,1024]{2,1,0:T(8,128)(2,1)S(1)}, bf16[2,320,1024]{2,1,0:T(8,128)(2,1)S(1)}, u32[]{:S(2)}, u32[]{:S(2)}) collective-permute-start(bf16[2,320,1024]{2,1,0:T(8,128)(2,1)S(1)} %unpack.1.own_ref), channel_id=1, source_target_pairs={{0,1},{1,0},{2,3},{3,2},{4,5},{5,4},{6,7},{7,6},{8,9},{9,8},{10,11... | collective-permute-start | bytes 3932168 | tf_op jit(solution)/shard_map/ppermute | solution.py:399
  72.7 0.0 copy-done
  72.7 0.0 copy-done.1
  72.7 0.0 copy-done.3
  72.7 0.7 half_products.1.half_ref
  73.4 1.9 %collective-permute-done.other_ref = bf16[2,320,1024]{2,1,0:T(8,128)(2,1)S(1)} collective-permute-done((bf16[2,320,1024]{2,1,0:T(8,128)(2,1)S(1)}, bf16[2,320,1024]{2,1,0:T(8,128)(2,1)S(1)}, u32[]{:S(2)}, u32[]{:S(2)}) %collective-permute-start) | collective-permute-done | bytes 1310752 | tf_op jit(solution)/shard_map/ppermute | solution.py:399
  75.3 1.5 %forward.1 = (bf16[8,328,128]{2,1,0:T(8,128)(2,1)S(1)}, bf16[3,320,128]{2,1,0:T(8,128)(2,1)S(1)}, bf16[8,128]{1,0:T(8,128)(2,1)S(1)}) custom-call(s32[1]{0:T(128)} %bitcast.2.core_s, f32[3,320,128]{2,1,0:T(8,128)S(1)} %half_products.1.half_ref, bf16[2,320,1024]{2,1,0:T(8,128)(2,1)S(1)} %collective-permute-done.other_ref, bf16[1,128,2048]{2,1,0:T(8,128)(2,1)S(1)} %copy-done, ...), custom_call_target="tpu_custom_call" | custom-call | tf_op jit(solution)/shard_map/forward/pallas_call | solution.py:256
  76.8 2.3 %collective-permute-start.1 = (bf16[8,328,128]{2,1,0:T(8,128)(2,1)S(1)}, bf16[8,328,128]{2,1,0:T(8,128)(2,1)S(1)}, u32[]{:S(2)}, u32[]{:S(2)}) collective-permute-start(bf16[8,328,128]{2,1,0:T(8,128)(2,1)S(1)} %get-tuple-element.25), channel_id=1, source_target_pairs={{0,1},{1,0},{2,3},{3,2},{4,5},{5,4},{6,7},{7,6},{8,9},{9,8},{10,11... | collective-permute-start | bytes 2015240 | tf_op jit(solution)/shard_map/ppermute | solution.py:399
  79.1 0.8 shared_sum.1
  79.8 0.5 keep_shares.1.keep_ref
  80.3 0.5 collective-permute-done.1.take_ref
  80.8 2.0 %back_rows.1 = bf16[512,8,128]{2,1,0:T(8,128)(2,1)S(1)} custom-call(bf16[8,328,128]{2,1,0:T(8,128)(2,1)S(1)} %keep_shares.1.keep_ref, bf16[8,328,128]{2,1,0:T(8,128)(2,1)S(1)} %collective-permute-done.1.take_ref, f32[8,128]{1,0:T(8,128)S(1)} %get-tuple-element.26.norm_ref), custom_call_target="tpu_custom_call" | custom-call | tf_op jit(solution)/shard_map/back_rows/pallas_call | solution.py:312
  82.8 0.0 copy-start.2
  82.8 1.0 copy-done.2
  83.8 22.6 %all-to-all-start.1 = ((bf16[512,8,128]{2,1,0:T(8,128)(2,1)}), bf16[512,8,128]{2,1,0:T(8,128)(2,1)}, u32[]{:S(2)}, u32[]{:S(2)}) async-start(bf16[512,8,128]{2,1,0:T(8,128)(2,1)} %copy-done.2), calls=%async_computation.1 | async-start | bytes 2097152 | tf_op jit(solution)/shard_map/all_to_all | solution.py:421
  106.4 0.0 copy-start.4
  106.4 0.0 copy-start.5
  106.4 1.9 %grads.1 = (bf16[1,128,2048]{2,1,0:T(8,128)(2,1)}, bf16[1,128,2048]{2,1,0:T(8,128)(2,1)}, bf16[1,128,2048]{2,1,0:T(8,128)(2,1)}, f32[3,1,128]{2,1,0:T(1,128)}) custom-call(s32[1]{0:T(128)} %bitcast.2.core_s, bf16[3,320,128]{2,1,0:T(8,128)(2,1)S(1)} %get-tuple-element.23.delta_ref, bf16[2,320,1024]{2,1,0:T(8,128)(2,1)S(1)} %unpack.1.own_ref, ...), custom_call_target="tpu_custom_call" | custom-call | tf_op jit(solution)/shard_map/grads/pallas_call | solution.py:345
  108.3 25.9 %all-to-all-done.1.recv_ref = bf16[512,8,128]{2,1,0:T(8,128)(2,1)} async-done(((bf16[512,8,128]{2,1,0:T(8,128)(2,1)}), bf16[512,8,128]{2,1,0:T(8,128)(2,1)}, u32[]{:S(2)}, u32[]{:S(2)}) %all-to-all-start.1) | async-done | bytes 1048608 | tf_op jit(solution)/shard_map/all_to_all | solution.py:421
  134.2 0.0 copy-done.4
  134.2 2.5 %end.1 = (bf16[128,128]{1,0:T(8,128)(2,1)}, f32[2,128]{1,0:T(2,128)}, f32[1,64]{1,0:T(1,128)}) custom-call(s32[1]{0:T(128)} %bitcast.at_s, s32[1]{0:T(128)} %bitcast.1.me_s, bf16[512,8,128]{2,1,0:T(8,128)(2,1)} %all-to-all-done.1.recv_ref, s32[2,128]{1,0:T(2,128)S(1)} %bitcast.10, s32[2,128]{1,0:T(2,128)S(1)} %get-tuple-element.27.rank_ref, ...), custom_call_target="tpu_custom_call" | custom-call | tf_op jit(solution)/shard_map/end/pallas_call | solution.py:384
  (4 shorter events, 0.0 us)
Async XLA Ops:
  66.9 5.8 %copy-start = (bf16[1,128,2048]{2,1,0:T(8,128)(2,1)S(1)}, bf16[1,128,2048]{2,1,0:T(8,128)(2,1)}, u32[]{:S(2)}) copy-start(bf16[1,128,2048]{2,1,0:T(8,128)(2,1)} %gate_ref.5) | copy-start | bytes 1572868
  66.9 5.8 %copy-start.1 = (bf16[1,128,2048]{2,1,0:T(8,128)(2,1)S(1)}, bf16[1,128,2048]{2,1,0:T(8,128)(2,1)}, u32[]{:S(2)}) copy-start(bf16[1,128,2048]{2,1,0:T(8,128)(2,1)} %up_ref.5) | copy-start | bytes 1572868
  66.9 5.8 %copy-start.3 = (bf16[1,128,2048]{2,1,0:T(8,128)(2,1)S(1)}, bf16[1,128,2048]{2,1,0:T(8,128)(2,1)}, u32[]{:S(2)}) copy-start(bf16[1,128,2048]{2,1,0:T(8,128)(2,1)} %down_ref.3) | copy-start | bytes 1572868
  67.6 7.7 %collective-permute-start = (bf16[2,320,1024]{2,1,0:T(8,128)(2,1)S(1)}, bf16[2,320,1024]{2,1,0:T(8,128)(2,1)S(1)}, u32[]{:S(2)}, u32[]{:S(2)}) collective-permute-start(bf16[2,320,1024]{2,1,0:T(8,128)(2,1)S(1)} %unpack.1.own_ref), channel_id=1, source_target_pairs={{0,1},{1,0},{2,3},{3,2},{4,5},{5,4},{6,7},{7,6},{8,9},{9,8},{10,11... | collective-permute-start | bytes 3932168 | tf_op jit(solution)/shard_map/ppermute | solution.py:399
  76.8 4.0 %collective-permute-start.1 = (bf16[8,328,128]{2,1,0:T(8,128)(2,1)S(1)}, bf16[8,328,128]{2,1,0:T(8,128)(2,1)S(1)}, u32[]{:S(2)}, u32[]{:S(2)}) collective-permute-start(bf16[8,328,128]{2,1,0:T(8,128)(2,1)S(1)} %get-tuple-element.25), channel_id=1, source_target_pairs={{0,1},{1,0},{2,3},{3,2},{4,5},{5,4},{6,7},{7,6},{8,9},{9,8},{10,11... | collective-permute-start | bytes 2015240 | tf_op jit(solution)/shard_map/ppermute | solution.py:399
  82.8 1.0 copy-start.2
  83.8 50.4 %all-to-all-start.1 = ((bf16[512,8,128]{2,1,0:T(8,128)(2,1)}), bf16[512,8,128]{2,1,0:T(8,128)(2,1)}, u32[]{:S(2)}, u32[]{:S(2)}) async-start(bf16[512,8,128]{2,1,0:T(8,128)(2,1)} %copy-done.2), calls=%async_computation.1 | async-start | bytes 2097152 | tf_op jit(solution)/shard_map/all_to_all | solution.py:421
  106.4 27.8 %copy-start.4 = (s32[128,2]{0,1:T(2,128)S(1)}, s32[128,2]{0,1:T(2,128)}, u32[]{:S(2)}) copy-start(s32[128,2]{0,1:T(2,128)} %param.10) | copy-start | bytes 3076
  106.4 27.8 %copy-start.5 = (f32[128,2]{0,1:T(2,128)S(1)}, f32[128,2]{0,1:T(2,128)}, u32[]{:S(2)}) copy-start(f32[128,2]{0,1:T(2,128)} %param.11) | copy-start | bytes 3076

commit v4 on v2

--- a/solution.py
+++ b/solution.py
@@ -422,9 +422,11 @@
     give, delta, inner = forward(core, half, other, gate_proj, up_proj, down_proj, cap)
     take = swap(give)
     keep = keep_shares(core, delta, inner, gate_proj, up_proj)
-    parts = lax.all_to_all(pair_sum(keep, take), "x", 0, 0, tiled=True)
+    summed, norms = lax.optimization_barrier((pair_sum(keep, take), norms))
+    parts = lax.all_to_all(summed, "x", 0, 0, tiled=True)
+    back = back_rows(parts, norms, n, cap)
+    back, delta = lax.optimization_barrier((back, delta))
     gate_grad, up_grad, down_grad, row_norms = grads(core, delta, own, other)
-    back = back_rows(parts, norms, n, cap)
     returned = lax.all_to_all(back, EP, 0, 0, tiled=True)
     token_grad, route_grad, shared_norms = end(me, returned, ids_t, rank, w_t, cap)
     return (

time: 131 us -> 129 us (0.985)
  blocking collectives: 62.8 us -> 89 us
  waiting for transfers between devices: 30.3 us -> 12.1 us
  starting transfers between devices: 21.2 us -> 14.8 us
  local copies, waits for them, and re-layouts: 4.43 us -> 0.02 us
    all_to_all x0 -> x1, blocking collectives: none -> 26.2 us  [local(): parts = lax.all_to_all(summed, 'x', 0, 0, tiled=True)]
    all_to_all x1 -> x0, waiting for transfers between devices: 19.8 us -> none  [local(): parts = lax.all_to_all(pair_sum(keep, take), 'x', 0, 0, tiled=True)]
    all_to_all x1 -> x0, starting transfers between devices: 6.49 us -> none  [local(): parts = lax.all_to_all(pair_sum(keep, take), 'x', 0, 0, tiled=True)]
    unnamed x28 -> x10, local copies, waits for them, and re-layouts: 4.43 us -> 0.02 us
    all_to_all x1, waiting for transfers between devices: 7.41 us -> 9.69 us  [local(): returned = lax.all_to_all(back, EP, 0, 0, tiled=True)]
  transfers between devices with their start and end apart: 4 -> 3, of which waited for: 4 -> 3; matrix products, arithmetic and copies ran while one was open for 0% -> 0% of each run, Pallas kernels for 3% -> 3%
where the time goes in v4:
time: 129 us; the launch traced here: 128 us
  blocking collectives  89 us (69%)
  starting transfers between devices  14.8 us (11%)
  waiting for transfers between devices  12.1 us (9%)
  Pallas kernels  11.3 us (9%)
    all_to_all x1, blocking collectives, local(): recv = lax.all_to_all(sent, EP, 0, 0, tiled=True)  62.8 us
    all_to_all x1, blocking collectives, local(): parts = lax.all_to_all(summed, 'x', 0, 0, tiled=True)  26.2 us
    all_to_all x1, waiting for transfers between devices, local(): returned = lax.all_to_all(back, EP, 0, 0, tiled=True)  9.69 us
    all_to_all x1, starting transfers between devices, local(): returned = lax.all_to_all(back, EP, 0, 0, tiled=True)  7.4 us
    ppermute x2, starting transfers between devices, swap(): return lax.ppermute(v, 'c', [(0, 1), (1, 0)])  7.38 us
    pallas_call x1, Pallas kernels, send_rows(): pl.pallas_call(functools.partial(send_kernel, cap), in_specs=in_smem(2) +...  3.37 us
  transfers between devices with their start and end apart: 3, of which 3 were waited for; matrix products, arithmetic and copies ran while one was open for 0% of the time, Pallas kernels for 3%

profile of v4, /device:TPU:1, one launch (start us, length us, event | category | flops | bytes accessed | tf_op | source)
XLA Modules:
  0.0 127.9 jit_solution(10274100587584345554)
XLA Ops:
  0.6 3.4 %send_rows.1 = (bf16[64,12,8,128]{3,2,1,0:T(8,128)(2,1)S(1)}, s32[2,128]{1,0:T(2,128)S(1)}) custom-call(s32[1]{0:T(128)} %bitcast.2.at_s, s32[1]{0:T(128)} %bitcast.me_s, bf16[128,2048]{1,0:T(8,128)(2,1)} %tok_ref.1, bf16[128,2048]{1,0:T(8,128)(2,1)} %grad_ref.1, bf16[128,1024]{1,0:T(8,128)(2,1)} %act_ref.1, s32[2,128]{1,0:T(2,128)} %bitcast.9, ...), custom_call_target="tpu_custom_call" | custom-call | tf_op jit(solution)/shard_map/send_rows/pallas_call | solution.py:122
  4.0 62.8 %all_to_all.15.recv_ref = bf16[64,12,8,128]{3,2,1,0:T(8,128)(2,1)S(1)} all-to-all(bf16[64,12,8,128]{3,2,1,0:T(8,128)(2,1)S(1)} %get-tuple-element.26), channel_id=1, replica_groups=mesh['z'=8,'y'=8,'x'=8,'c'=2] {'z','y'}, dimensions={0} | all-to-all | bytes 3145728 | tf_op jit(solution)/shard_map/all_to_all | solution.py:417
  66.9 0.0 copy-start
  66.9 0.7 unpack.1.own_ref
  67.6 5.1 %collective-permute-start = (bf16[2,320,1024]{2,1,0:T(8,128)(2,1)S(1)}, bf16[2,320,1024]{2,1,0:T(8,128)(2,1)S(1)}, u32[]{:S(2)}, u32[]{:S(2)}) collective-permute-start(bf16[2,320,1024]{2,1,0:T(8,128)(2,1)S(1)} %unpack.1.own_ref), channel_id=1, source_target_pairs={{0,1},{1,0},{2,3},{3,2},{4,5},{5,4},{6,7},{7,6},{8,9},{9,8},{10,11... | collective-permute-start | bytes 3932168 | tf_op jit(solution)/shard_map/ppermute | solution.py:404
  72.7 0.0 copy-done
  72.7 0.0 copy-done.1
  72.7 0.0 copy-done.2
  72.7 0.7 half_products.1.half_ref
  73.4 1.9 %collective-permute-done.other_ref = bf16[2,320,1024]{2,1,0:T(8,128)(2,1)S(1)} collective-permute-done((bf16[2,320,1024]{2,1,0:T(8,128)(2,1)S(1)}, bf16[2,320,1024]{2,1,0:T(8,128)(2,1)S(1)}, u32[]{:S(2)}, u32[]{:S(2)}) %collective-permute-start) | collective-permute-done | bytes 1310752 | tf_op jit(solution)/shard_map/ppermute | solution.py:404
  75.3 1.5 %forward.1 = (bf16[8,328,128]{2,1,0:T(8,128)(2,1)S(1)}, bf16[3,320,128]{2,1,0:T(8,128)(2,1)S(1)}, bf16[8,128]{1,0:T(8,128)(2,1)S(1)}) custom-call(s32[1]{0:T(128)} %bitcast.1.core_s, f32[3,320,128]{2,1,0:T(8,128)S(1)} %half_products.1.half_ref, bf16[2,320,1024]{2,1,0:T(8,128)(2,1)S(1)} %collective-permute-done.other_ref, bf16[1,128,2048]{2,1,0:T(8,128)(2,1)S(1)} %copy-done, ...), custom_call_target="tpu_custom_call" | custom-call | tf_op jit(solution)/shard_map/forward/pallas_call | solution.py:256
  76.8 2.3 %collective-permute-start.1 = (bf16[8,328,128]{2,1,0:T(8,128)(2,1)S(1)}, bf16[8,328,128]{2,1,0:T(8,128)(2,1)S(1)}, u32[]{:S(2)}, u32[]{:S(2)}) collective-permute-start(bf16[8,328,128]{2,1,0:T(8,128)(2,1)S(1)} %get-tuple-element.29), channel_id=1, source_target_pairs={{0,1},{1,0},{2,3},{3,2},{4,5},{5,4},{6,7},{7,6},{8,9},{9,8},{10,11... | collective-permute-start | bytes 2015240 | tf_op jit(solution)/shard_map/ppermute | solution.py:404
  79.1 0.8 shared_sum.1
  79.8 0.5 keep_shares.1.a_ref
  80.4 0.5 collective-permute-done.1.b_ref
  80.8 0.2 pair_sum.1
  81.0 26.2 %all_to_all.16.parts_ref = bf16[8,328,128]{2,1,0:T(8,128)(2,1)S(1)} all-to-all(bf16[8,328,128]{2,1,0:T(8,128)(2,1)S(1)} %pair_sum.1), channel_id=1, replica_groups=mesh['z'=8,'y'=8,'x'=8,'c'=2] {'x'}, dimensions={0} | all-to-all | bytes 1343488 | tf_op jit(solution)/shard_map/all_to_all | solution.py:426
  107.1 0.8 back_rows.1
  108.0 7.4 %all-to-all-start.2 = ((bf16[64,8,128]{2,1,0:T(8,128)(2,1)}), bf16[64,8,128]{2,1,0:T(8,128)(2,1)S(1)}, u32[]{:S(2)}, u32[]{:S(2)}) async-start(bf16[64,8,128]{2,1,0:T(8,128)(2,1)} %back_rows.1), calls=%async_computation.2 | async-start | bytes 262144 | tf_op jit(solution)/shard_map/all_to_all | solution.py:430
  115.4 1.9 %grads.1 = (bf16[1,128,2048]{2,1,0:T(8,128)(2,1)}, bf16[1,128,2048]{2,1,0:T(8,128)(2,1)}, bf16[1,128,2048]{2,1,0:T(8,128)(2,1)}, f32[3,1,128]{2,1,0:T(1,128)}) custom-call(s32[1]{0:T(128)} %bitcast.1.core_s, bf16[3,320,128]{2,1,0:T(8,128)(2,1)S(1)} %get-tuple-element.37.delta_ref, bf16[2,320,1024]{2,1,0:T(8,128)(2,1)S(1)} %unpack.1.own_ref, ...), custom_call_target="tpu_custom_call" | custom-call | tf_op jit(solution)/shard_map/grads/pallas_call | solution.py:320
  117.2 9.7 %all-to-all-done.2.recv_ref = bf16[64,8,128]{2,1,0:T(8,128)(2,1)S(1)} async-done(((bf16[64,8,128]{2,1,0:T(8,128)(2,1)}), bf16[64,8,128]{2,1,0:T(8,128)(2,1)S(1)}, u32[]{:S(2)}, u32[]{:S(2)}) %all-to-all-start.2) | async-done | bytes 131104 | tf_op jit(solution)/shard_map/all_to_all | solution.py:430
  126.9 0.0 copy-done.3
  126.9 0.0 copy-done.4
  126.9 0.9 end.1
  (4 shorter events, 0.0 us)
Async XLA Ops:
  66.9 5.8 %copy-start = (bf16[1,128,2048]{2,1,0:T(8,128)(2,1)S(1)}, bf16[1,128,2048]{2,1,0:T(8,128)(2,1)}, u32[]{:S(2)}) copy-start(bf16[1,128,2048]{2,1,0:T(8,128)(2,1)} %gate_ref.5) | copy-start | bytes 1572868
  66.9 5.8 %copy-start.1 = (bf16[1,128,2048]{2,1,0:T(8,128)(2,1)S(1)}, bf16[1,128,2048]{2,1,0:T(8,128)(2,1)}, u32[]{:S(2)}) copy-start(bf16[1,128,2048]{2,1,0:T(8,128)(2,1)} %up_ref.5) | copy-start | bytes 1572868
  66.9 5.8 %copy-start.2 = (bf16[1,128,2048]{2,1,0:T(8,128)(2,1)S(1)}, bf16[1,128,2048]{2,1,0:T(8,128)(2,1)}, u32[]{:S(2)}) copy-start(bf16[1,128,2048]{2,1,0:T(8,128)(2,1)} %down_ref.3) | copy-start | bytes 1572868
  67.6 7.7 %collective-permute-start = (bf16[2,320,1024]{2,1,0:T(8,128)(2,1)S(1)}, bf16[2,320,1024]{2,1,0:T(8,128)(2,1)S(1)}, u32[]{:S(2)}, u32[]{:S(2)}) collective-permute-start(bf16[2,320,1024]{2,1,0:T(8,128)(2,1)S(1)} %unpack.1.own_ref), channel_id=1, source_target_pairs={{0,1},{1,0},{2,3},{3,2},{4,5},{5,4},{6,7},{7,6},{8,9},{9,8},{10,11... | collective-permute-start | bytes 3932168 | tf_op jit(solution)/shard_map/ppermute | solution.py:404
  76.8 4.0 %collective-permute-start.1 = (bf16[8,328,128]{2,1,0:T(8,128)(2,1)S(1)}, bf16[8,328,128]{2,1,0:T(8,128)(2,1)S(1)}, u32[]{:S(2)}, u32[]{:S(2)}) collective-permute-start(bf16[8,328,128]{2,1,0:T(8,128)(2,1)S(1)} %get-tuple-element.29), channel_id=1, source_target_pairs={{0,1},{1,0},{2,3},{3,2},{4,5},{5,4},{6,7},{7,6},{8,9},{9,8},{10,11... | collective-permute-start | bytes 2015240 | tf_op jit(solution)/shard_map/ppermute | solution.py:404
  108.0 19.0 %copy-start.3 = (s32[128,2]{0,1:T(2,128)S(1)}, s32[128,2]{0,1:T(2,128)}, u32[]{:S(2)}) copy-start(s32[128,2]{0,1:T(2,128)} %param.10) | copy-start | bytes 3076
  108.0 19.0 %copy-start.4 = (f32[128,2]{0,1:T(2,128)S(1)}, f32[128,2]{0,1:T(2,128)}, u32[]{:S(2)}) copy-start(f32[128,2]{0,1:T(2,128)} %param.11) | copy-start | bytes 3076
  108.0 19.0 %all-to-all-start.2 = ((bf16[64,8,128]{2,1,0:T(8,128)(2,1)}), bf16[64,8,128]{2,1,0:T(8,128)(2,1)S(1)}, u32[]{:S(2)}, u32[]{:S(2)}) async-start(bf16[64,8,128]{2,1,0:T(8,128)(2,1)} %back_rows.1), calls=%async_computation.2 | async-start | bytes 262144 | tf_op jit(solution)/shard_map/all_to_all | solution.py:430

commit v5 on v2

--- a/solution.py
+++ b/solution.py
@@ -84,21 +84,6 @@
     spread(tok_t, tok_v[...])
     spread(grad_t, grad_v[:, mine])
 
-    def one_token(t, carry):
-        rows = pl.ds(pl.multiple_of(t * TILE, TILE), TILE)
-        tok = tok_t[rows, :].astype(BF)
-        grad = grad_t[rows, :]
-        for k in range(2):
-            e = ids_s[k, t]
-            r = seen_s[e]
-            seen_s[e] = r + 1
-            rank_s[k, t] = r
-            out_ref[e, r] = tok
-            out_ref[e, cap + r] = (w_s[k, t] * grad).astype(BF)
-        return carry
-
-    lax.fori_loop(0, count, one_token, 0, unroll=8)
-
     half = LANES // 2
     act = act_v[...]
     swapped = jnp.concatenate([act[:, half:], act[:, :half]], axis=1)
@@ -107,14 +92,30 @@
     twice = jnp.where(keep, act.astype(F32), swapped.astype(F32)).astype(BF)
     step = 2 * LANES
     block = width // experts
-    for s in range(0, width, step):
-        term = dot(grad_v[:, s : s + step], twice, 0, 0)
-        term = term.reshape(step // block, 2, block // 2, LANES)
-        lane = iota((step // block, block // 2, LANES), 2)
-        both = jnp.where(lane < half, term[:, 0], term[:, 1]).astype(BF)
-        out_ref[s // block : (s + step) // block, 2 * cap :] = both.reshape(
-            step // block, SHARED, TILE, LANES
-        )
+    n = step // block
+    steps = width // step
+
+    def one_step(i, carry):
+        for j in range(count // steps):
+            t = i * (count // steps) + j
+            rows = pl.ds(pl.multiple_of(t * TILE, TILE), TILE)
+            tok = tok_t[rows, :].astype(BF)
+            grad = grad_t[rows, :]
+            for k in range(2):
+                e = ids_s[k, t]
+                r = seen_s[e]
+                seen_s[e] = r + 1
+                rank_s[k, t] = r
+                out_ref[e, r] = tok
+                out_ref[e, cap + r] = (w_s[k, t] * grad).astype(BF)
+        cols = pl.ds(pl.multiple_of(i * step, step), step)
+        term = dot(grad_v[:, cols], twice, 0, 0).reshape(n, 2, block // 2, LANES)
+        left = iota((n, block // 2, LANES), 2) < half
+        both = jnp.where(left, term[:, 0], term[:, 1]).astype(BF)
+        out_ref[pl.ds(i * n, n), 2 * cap :] = both.reshape(n, SHARED, TILE, LANES)
+        return carry
+
+    lax.fori_loop(0, steps, one_step, 0)
 
 
 def send_rows(at, me, tokens, out_grad, act, ids_t, w_t, cap, experts):
@@ -200,34 +201,36 @@
     return sums
 
 
-def half_kernel(core_s, own_ref, gate_ref, up_ref, down_ref, out_ref):
+def columns(ref, x, side):
+    return ref[0, :, pl.ds(pl.multiple_of((2 * x + side) * LANES, LANES), LANES)]
+
+
+def half_kernel(core_s, own_ref, gate_ref, up_ref, down_ref, out_ref, give_ref):
+    for x in range(give_ref.shape[1] // LANES):
+        pair = [columns(ref, x, 1 - core_s[0]) for ref in (gate_ref, up_ref)]
+        give_ref[:, x * LANES : (x + 1) * LANES] = jnp.concatenate(pair, axis=0)
     sums = products(core_s[0], own_ref, gate_ref, up_ref, down_ref, [0.0] * 3)
     for k in range(3):
         out_ref[k] = sums[k]
 
 
 def half_products(core, own, gate, up, down):
+    feats = gate.shape[1]
     return pl.pallas_call(
         half_kernel,
         in_specs=in_smem(1) + in_vmem(4),
-        out_specs=pl.BlockSpec(memory_space=pltpu.VMEM),
-        out_shape=jax.ShapeDtypeStruct((3, own.shape[1], gate.shape[1]), F32),
+        out_specs=in_vmem(2),
+        out_shape=[
+            jax.ShapeDtypeStruct((3, own.shape[1], feats), F32),
+            jax.ShapeDtypeStruct((2 * feats, HALF), BF),
+        ],
         compiler_params=params(16),
         name="half_products",
     )(core, own, gate, up, down)
 
 
-def shares(side, deltas, gate_ref, up_ref, inner, ref):
-    count = deltas.shape[0]
-    for j in range(ref.shape[0]):
-        cols = pl.ds(pl.multiple_of(j * 2 * LANES + side * LANES, LANES), LANES)
-        w = jnp.concatenate([gate_ref[0, :, cols], up_ref[0, :, cols]], axis=0)
-        ref[j, :count] = dot(deltas, w).astype(BF)
-        ref[j, count:] = inner
-
-
 def forward_kernel(
-    cap, core_s, half_ref, other_ref, gate_ref, up_ref, down_ref, give_ref, delta_ref, inner_ref
+    cap, core_s, half_ref, other_ref, gate_ref, up_ref, down_ref, give_ref, hidden_ref
 ):
     core = core_s[0]
     count = other_ref.shape[1]
@@ -236,74 +239,73 @@
     sig = jax.nn.sigmoid(gate_pre)
     silu = gate_pre * sig
     hidden = (silu * up_pre).astype(BF)
+    hidden_ref[...] = hidden
     up_delta = (hidden_grad * silu).astype(BF)
     gate_delta = (hidden_grad * up_pre * sig * (1.0 + gate_pre * (1.0 - sig))).astype(BF)
+    give_ref[:count] = gate_delta
+    give_ref[count : 2 * count] = up_delta
     inner = jnp.sum(hidden.astype(F32) * hidden_grad, axis=1, keepdims=True)
     slot = iota((count, LANES), 0)
     lane = (slot // cap) % GROUP * TILE + slot % cap
     spots = jnp.where(lane == iota((count, LANES), 1), inner, 0.0)
     span = GROUP * cap
     lines = [jnp.sum(spots[s : s + span], axis=0, keepdims=True) for s in range(0, count, span)]
-    tile = jnp.concatenate(split2(jnp.concatenate(lines, axis=0)), axis=0).astype(BF)
-    inner_ref[...] = tile
-    shares(1 - core, jnp.concatenate([gate_delta, up_delta], axis=1), gate_ref, up_ref, tile, give_ref)
-    for k, d in enumerate((gate_delta, up_delta, hidden)):
-        delta_ref[k] = d
+    tile = jnp.concatenate(split2(jnp.concatenate(lines, axis=0)), axis=0)
+    give_ref[2 * count :] = tile.astype(BF)
 
 
 def forward(core, half, other, gate, up, down, cap):
     count = other.shape[1]
+    feats = gate.shape[1]
     return pl.pallas_call(
         functools.partial(forward_kernel, cap),
         in_specs=in_smem(1) + in_vmem(5),
-        out_specs=in_vmem(3),
+        out_specs=in_vmem(2),
         out_shape=[
-            jax.ShapeDtypeStruct((TILE, count + TILE, LANES), BF),
-            jax.ShapeDtypeStruct((3, count, gate.shape[1]), BF),
-            jax.ShapeDtypeStruct((TILE, LANES), BF),
+            jax.ShapeDtypeStruct((2 * count + TILE, feats), BF),
+            jax.ShapeDtypeStruct((count, feats), BF),
         ],
         compiler_params=params(24),
         name="forward",
     )(core, half, other, gate, up, down)
 
 
-def keep_kernel(core_s, delta_ref, inner_ref, gate_ref, up_ref, keep_ref):
-    deltas = jnp.concatenate([delta_ref[0], delta_ref[1]], axis=1)
-    shares(core_s[0], deltas, gate_ref, up_ref, inner_ref[...], keep_ref)
-
-
-def keep_shares(core, delta, inner, gate, up):
-    return pl.pallas_call(
-        keep_kernel,
-        in_specs=in_smem(1) + in_vmem(4),
+def shares_kernel(core_s, give_ref, take_ref, cols_ref, gate_ref, up_ref, out_ref):
+    count = (give_ref.shape[0] - TILE) // 2
+    deltas = [ref[k * count : (k + 1) * count] for ref in (give_ref, take_ref) for k in range(2)]
+    deltas = jnp.concatenate(deltas, axis=1)
+    last = give_ref[2 * count :].astype(F32) + take_ref[2 * count :].astype(F32)
+    inner = split2(last[: TILE // 2] + last[TILE // 2 :])
+    inner = jnp.concatenate(inner, axis=0).astype(BF)
+    for x in range(out_ref.shape[0]):
+        pair = [columns(ref, x, core_s[0]) for ref in (gate_ref, up_ref)]
+        pair.append(cols_ref[:, x * LANES : (x + 1) * LANES])
+        out_ref[x, :count] = dot(deltas, jnp.concatenate(pair, axis=0)).astype(BF)
+        out_ref[x, count:] = inner
+
+
+def shares(core, give, take, cols, gate, up):
+    count = (give.shape[0] - TILE) // 2
+    return pl.pallas_call(
+        shares_kernel,
+        in_specs=in_smem(1) + in_vmem(5),
         out_specs=pl.BlockSpec(memory_space=pltpu.VMEM),
-        out_shape=jax.ShapeDtypeStruct((TILE, delta.shape[1] + TILE, LANES), BF),
-        compiler_params=params(16),
-        name="keep_shares",
-    )(core, delta, inner, gate, up)
-
-
-def pair_kernel(a_ref, b_ref, out_ref):
-    out_ref[...] = (a_ref[...].astype(F32) + b_ref[...].astype(F32)).astype(BF)
-
-
-def pair_sum(a, b):
-    return pl.pallas_call(
-        pair_kernel,
-        in_specs=in_vmem(2),
-        out_specs=pl.BlockSpec(memory_space=pltpu.VMEM),
-        out_shape=jax.ShapeDtypeStruct(a.shape, BF),
-        compiler_params=params(16),
-        name="pair_sum",
-    )(a, b)
-
-
-def grads_kernel(core_s, delta_ref, own_ref, other_ref, gate_ref, up_ref, down_ref, norm_ref):
+        out_shape=jax.ShapeDtypeStruct((TILE, count + TILE, LANES), BF),
+        compiler_params=params(16),
+        name="shares",
+    )(core, give, take, cols, gate, up)
+
+
+def grads_kernel(
+    core_s, give_ref, hidden_ref, own_ref, other_ref, gate_ref, up_ref, down_ref, norm_ref
+):
     core = core_s[0]
+    count = hidden_ref.shape[0]
+    deltas = (give_ref[:count], give_ref[count : 2 * count], hidden_ref[...])
     step = 2 * LANES
     for k, (out, which) in enumerate(((gate_ref, 0), (up_ref, 0), (down_ref, 1))):
         total = 0.0
-        delta = delta_ref[k].astype(F32).T.astype(BF)
+        delta = deltas[k].astype(F32).T.astype(BF)
         for side, ref in ((core, own_ref), (1 - core, other_ref)):
             for s in range(0, HALF, step):
                 g = dot(delta, ref[which, :, s : s + step])
@@ -314,17 +316,17 @@
         norm_ref[k] = jnp.sum(total.T, axis=0, keepdims=True)
 
 
-def grads(core, delta, own, other):
-    feats = delta.shape[2]
+def grads(core, give, hidden, own, other):
+    feats = hidden.shape[1]
     out = jax.ShapeDtypeStruct((1, feats, 2 * HALF), BF)
     return pl.pallas_call(
         grads_kernel,
-        in_specs=in_smem(1) + in_vmem(3),
+        in_specs=in_smem(1) + in_vmem(4),
         out_specs=in_vmem(4),
         out_shape=[out, out, out, jax.ShapeDtypeStruct((3, 1, feats), F32)],
         compiler_params=params(24),
         name="grads",
-    )(core, delta, own, other)
+    )(core, give, hidden, own, other)
 
 
 def back_kernel(cap, parts_ref, norm_ref, out_ref, sums, rows):
@@ -417,14 +419,15 @@
     recv = lax.all_to_all(sent, EP, 0, 0, tiled=True)
     own = unpack(recv, cap)
     other = swap(own)
-    half = half_products(core, own, gate_proj, up_proj, down_proj)
+    half, cols = half_products(core, own, gate_proj, up_proj, down_proj)
+    cols = swap(cols)
     shared, norms = shared_sum(recv, cap)
-    give, delta, inner = forward(core, half, other, gate_proj, up_proj, down_proj, cap)
-    take = swap(give)
-    keep = keep_shares(core, delta, inner, gate_proj, up_proj)
-    parts = lax.all_to_all(pair_sum(keep, take), "x", 0, 0, tiled=True)
-    gate_grad, up_grad, down_grad, row_norms = grads(core, delta, own, other)
-    back = back_rows(parts, norms, n, cap)
+    give, hidden = forward(core, half, other, gate_proj, up_proj, down_proj, cap)
+    part = shares(core, give, swap(give), cols, gate_proj, up_proj)
+    part, norms = lax.optimization_barrier((part, norms))
+    back = back_rows(lax.all_to_all(part, "x", 0, 0, tiled=True), norms, n, cap)
+    back, hidden = lax.optimization_barrier((back, hidden))
+    gate_grad, up_grad, down_grad, row_norms = grads(core, give, hidden, own, other)
     returned = lax.all_to_all(back, EP, 0, 0, tiled=True)
     token_grad, route_grad, shared_norms = end(me, returned, ids_t, rank, w_t, cap)
     return (

time: 131 us -> 129 us (0.985)
  blocking collectives: 62.8 us -> 89 us
  waiting for transfers between devices: 30.3 us -> 9.94 us
  local copies, waits for them, and re-layouts: 4.43 us -> 0.02 us
  starting transfers between devices: 21.2 us -> 16.8 us
    all_to_all x0 -> x1, blocking collectives: none -> 26.2 us  [local(): back = back_rows(lax.all_to_all(part, 'x', 0, 0, tiled=True), norms, n, cap)]
    all_to_all x1 -> x0, waiting for transfers between devices: 19.8 us -> none  [local(): parts = lax.all_to_all(pair_sum(keep, take), 'x', 0, 0, tiled=True)]
    all_to_all x1 -> x0, starting transfers between devices: 6.49 us -> none  [local(): parts = lax.all_to_all(pair_sum(keep, take), 'x', 0, 0, tiled=True)]
    unnamed x28 -> x10, local copies, waits for them, and re-layouts: 4.43 us -> 0.02 us
    ppermute x2 -> x3, waiting for transfers between devices: 3.11 us -> 0.26 us  [swap(): return lax.ppermute(v, 'c', [(0, 1), (1, 0)])]
    all_to_all x1, waiting for transfers between devices: 7.41 us -> 9.68 us  [local(): returned = lax.all_to_all(back, EP, 0, 0, tiled=True)]
    ppermute x2 -> x3, starting transfers between devices: 7.38 us -> 9.42 us  [swap(): return lax.ppermute(v, 'c', [(0, 1), (1, 0)])]
    pallas_call x4 -> x3, Pallas kernels: 3.22 us -> 3.51 us  [the longest x1 1.87 us: grads(): pl.pallas_call(grads_kernel, in_specs=in_smem(1) + in_vmem(4), out_specs=...]
  transfers between devices with their start and end apart: 4 -> 4, of which waited for: 4 -> 2; matrix products, arithmetic and copies ran while one was open for 0% -> 0% of each run, Pallas kernels for 3% -> 3%
where the time goes in v5:
time: 129 us; the launch traced here: 128 us
  blocking collectives  89 us (69%)
  starting transfers between devices  16.8 us (13%)
  Pallas kernels  11.3 us (9%)
  waiting for transfers between devices  9.94 us (8%)
    all_to_all x1, blocking collectives, local(): recv = lax.all_to_all(sent, EP, 0, 0, tiled=True)  62.8 us
    all_to_all x1, blocking collectives, local(): back = back_rows(lax.all_to_all(part, 'x', 0, 0, tiled=True), norms, n, cap)  26.2 us
    all_to_all x1, waiting for transfers between devices, local(): returned = lax.all_to_all(back, EP, 0, 0, tiled=True)  9.68 us
    ppermute x3, starting transfers between devices, swap(): return lax.ppermute(v, 'c', [(0, 1), (1, 0)])  9.42 us
    all_to_all x1, starting transfers between devices, local(): returned = lax.all_to_all(back, EP, 0, 0, tiled=True)  7.39 us
    pallas_call x1, Pallas kernels, send_rows(): pl.pallas_call(functools.partial(send_kernel, cap), in_specs=in_smem(2) +...  3.73 us
  transfers between devices with their start and end apart: 4, of which 2 were waited for; matrix products, arithmetic and copies ran while one was open for 0% of the time, Pallas kernels for 3%

profile of v5, /device:TPU:1, one launch (start us, length us, event | category | flops | bytes accessed | tf_op | source)
XLA Modules:
  0.0 127.8 jit_solution(11300465887381145315)
XLA Ops:
  0.6 3.7 %send_rows.1 = (bf16[64,12,8,128]{3,2,1,0:T(8,128)(2,1)S(1)}, s32[2,128]{1,0:T(2,128)S(1)}) custom-call(s32[1]{0:T(128)} %bitcast.2.at_s, s32[1]{0:T(128)} %bitcast.me_s, bf16[128,2048]{1,0:T(8,128)(2,1)} %tok_ref.1, bf16[128,2048]{1,0:T(8,128)(2,1)} %grad_ref.1, bf16[128,1024]{1,0:T(8,128)(2,1)} %act_ref.1, s32[2,128]{1,0:T(2,128)} %bitcast.9, ...), custom_call_target="tpu_custom_call" | custom-call | tf_op jit(solution)/shard_map/send_rows/pallas_call | solution.py:123
  4.4 62.8 %all_to_all.15.recv_ref = bf16[64,12,8,128]{3,2,1,0:T(8,128)(2,1)S(1)} all-to-all(bf16[64,12,8,128]{3,2,1,0:T(8,128)(2,1)S(1)} %get-tuple-element.27), channel_id=1, replica_groups=mesh['z'=8,'y'=8,'x'=8,'c'=2] {'z','y'}, dimensions={0} | all-to-all | bytes 3145728 | tf_op jit(solution)/shard_map/all_to_all | solution.py:419
  67.2 0.7 unpack.1.own_ref
  67.9 5.1 %collective-permute-start = (bf16[2,320,1024]{2,1,0:T(8,128)(2,1)S(1)}, bf16[2,320,1024]{2,1,0:T(8,128)(2,1)S(1)}, u32[]{:S(2)}, u32[]{:S(2)}) collective-permute-start(bf16[2,320,1024]{2,1,0:T(8,128)(2,1)S(1)} %unpack.1.own_ref), channel_id=1, source_target_pairs={{0,1},{1,0},{2,3},{3,2},{4,5},{5,4},{6,7},{7,6},{8,9},{9,8},{10,11... | collective-permute-start | bytes 3932168 | tf_op jit(solution)/shard_map/ppermute | solution.py:406
  73.0 0.0 copy-done
  73.0 0.0 copy-done.1
  73.0 0.0 copy-done.2
  73.1 0.8 half_products.1
  73.8 1.9 %collective-permute-start.2 = (bf16[256,1024]{1,0:T(8,128)(2,1)S(1)}, bf16[256,1024]{1,0:T(8,128)(2,1)S(1)}, u32[]{:S(2)}, u32[]{:S(2)}) collective-permute-start(bf16[256,1024]{1,0:T(8,128)(2,1)S(1)} %get-tuple-element.30), channel_id=1, source_target_pairs={{0,1},{1,0},{2,3},{3,2},{4,5},{5,4},{6,7},{7,6},{8,9},{9,8},{10,11... | collective-permute-start | bytes 1572872 | tf_op jit(solution)/shard_map/ppermute | solution.py:406
  75.8 0.0 collective-permute-done.other_ref
  75.8 0.8 forward.1
  76.6 2.4 %collective-permute-start.1 = (bf16[648,128]{1,0:T(8,128)(2,1)S(1)}, bf16[648,128]{1,0:T(8,128)(2,1)S(1)}, u32[]{:S(2)}, u32[]{:S(2)}) collective-permute-start(bf16[648,128]{1,0:T(8,128)(2,1)S(1)} %get-tuple-element.29.give_ref), channel_id=1, source_target_pairs={{0,1},{1,0},{2,3},{3,2},{4,5},{5,4},{6,7},{7,6},{8,9},{9,8},{10,11... | collective-permute-start | bytes 497672 | tf_op jit(solution)/shard_map/ppermute | solution.py:406
  79.0 0.8 shared_sum.1
  79.8 0.0 collective-permute-done.2.cols_ref
  79.8 0.3 collective-permute-done.1.take_ref
  80.0 0.9 shares.1
  80.9 26.2 %all_to_all.16.parts_ref = bf16[8,328,128]{2,1,0:T(8,128)(2,1)S(1)} all-to-all(bf16[8,328,128]{2,1,0:T(8,128)(2,1)S(1)} %shares.1), channel_id=1, replica_groups=mesh['z'=8,'y'=8,'x'=8,'c'=2] {'x'}, dimensions={0} | all-to-all | bytes 1343488 | tf_op jit(solution)/shard_map/all_to_all | solution.py:428
  107.1 0.8 back_rows.1
  108.0 7.4 %all-to-all-start.2 = ((bf16[64,8,128]{2,1,0:T(8,128)(2,1)}), bf16[64,8,128]{2,1,0:T(8,128)(2,1)S(1)}, u32[]{:S(2)}, u32[]{:S(2)}) async-start(bf16[64,8,128]{2,1,0:T(8,128)(2,1)} %back_rows.1), calls=%async_computation.2 | async-start | bytes 262144 | tf_op jit(solution)/shard_map/all_to_all | solution.py:431
  115.4 1.9 %grads.1 = (bf16[1,128,2048]{2,1,0:T(8,128)(2,1)}, bf16[1,128,2048]{2,1,0:T(8,128)(2,1)}, bf16[1,128,2048]{2,1,0:T(8,128)(2,1)}, f32[3,1,128]{2,1,0:T(1,128)}) custom-call(s32[1]{0:T(128)} %bitcast.1.core_s, bf16[648,128]{1,0:T(8,128)(2,1)S(1)} %get-tuple-element.29.give_ref, bf16[320,128]{1,0:T(8,128)(2,1)S(1)} %get-tuple-element.39.hidden_ref, ...), custom_call_target="tpu_custom_call" | custom-call | tf_op jit(solution)/shard_map/grads/pallas_call | solution.py:322
  117.2 9.7 %all-to-all-done.2.recv_ref = bf16[64,8,128]{2,1,0:T(8,128)(2,1)S(1)} async-done(((bf16[64,8,128]{2,1,0:T(8,128)(2,1)}), bf16[64,8,128]{2,1,0:T(8,128)(2,1)S(1)}, u32[]{:S(2)}, u32[]{:S(2)}) %all-to-all-start.2) | async-done | bytes 131104 | tf_op jit(solution)/shard_map/all_to_all | solution.py:431
  126.9 0.0 copy-done.3
  126.9 0.0 copy-done.4
  126.9 0.9 end.1
  (5 shorter events, 0.0 us)
Async XLA Ops:
  67.2 5.8 %copy-start = (bf16[1,128,2048]{2,1,0:T(8,128)(2,1)S(1)}, bf16[1,128,2048]{2,1,0:T(8,128)(2,1)}, u32[]{:S(2)}) copy-start(bf16[1,128,2048]{2,1,0:T(8,128)(2,1)} %gate_ref.5) | copy-start | bytes 1572868
  67.2 5.8 %copy-start.1 = (bf16[1,128,2048]{2,1,0:T(8,128)(2,1)S(1)}, bf16[1,128,2048]{2,1,0:T(8,128)(2,1)}, u32[]{:S(2)}) copy-start(bf16[1,128,2048]{2,1,0:T(8,128)(2,1)} %up_ref.5) | copy-start | bytes 1572868
  67.2 5.8 %copy-start.2 = (bf16[1,128,2048]{2,1,0:T(8,128)(2,1)S(1)}, bf16[1,128,2048]{2,1,0:T(8,128)(2,1)}, u32[]{:S(2)}) copy-start(bf16[1,128,2048]{2,1,0:T(8,128)(2,1)} %down_ref.3) | copy-start | bytes 1572868
  67.9 7.8 %collective-permute-start = (bf16[2,320,1024]{2,1,0:T(8,128)(2,1)S(1)}, bf16[2,320,1024]{2,1,0:T(8,128)(2,1)S(1)}, u32[]{:S(2)}, u32[]{:S(2)}) collective-permute-start(bf16[2,320,1024]{2,1,0:T(8,128)(2,1)S(1)} %unpack.1.own_ref), channel_id=1, source_target_pairs={{0,1},{1,0},{2,3},{3,2},{4,5},{5,4},{6,7},{7,6},{8,9},{9,8},{10,11... | collective-permute-start | bytes 3932168 | tf_op jit(solution)/shard_map/ppermute | solution.py:406
  73.8 6.0 %collective-permute-start.2 = (bf16[256,1024]{1,0:T(8,128)(2,1)S(1)}, bf16[256,1024]{1,0:T(8,128)(2,1)S(1)}, u32[]{:S(2)}, u32[]{:S(2)}) collective-permute-start(bf16[256,1024]{1,0:T(8,128)(2,1)S(1)} %get-tuple-element.30), channel_id=1, source_target_pairs={{0,1},{1,0},{2,3},{3,2},{4,5},{5,4},{6,7},{7,6},{8,9},{9,8},{10,11... | collective-permute-start | bytes 1572872 | tf_op jit(solution)/shard_map/ppermute | solution.py:406
  76.6 3.4 %collective-permute-start.1 = (bf16[648,128]{1,0:T(8,128)(2,1)S(1)}, bf16[648,128]{1,0:T(8,128)(2,1)S(1)}, u32[]{:S(2)}, u32[]{:S(2)}) collective-permute-start(bf16[648,128]{1,0:T(8,128)(2,1)S(1)} %get-tuple-element.29.give_ref), channel_id=1, source_target_pairs={{0,1},{1,0},{2,3},{3,2},{4,5},{5,4},{6,7},{7,6},{8,9},{9,8},{10,11... | collective-permute-start | bytes 497672 | tf_op jit(solution)/shard_map/ppermute | solution.py:406
  108.0 19.0 %copy-start.3 = (s32[128,2]{0,1:T(2,128)S(1)}, s32[128,2]{0,1:T(2,128)}, u32[]{:S(2)}) copy-start(s32[128,2]{0,1:T(2,128)} %param.10) | copy-start | bytes 3076
  108.0 19.0 %copy-start.4 = (f32[128,2]{0,1:T(2,128)S(1)}, f32[128,2]{0,1:T(2,128)}, u32[]{:S(2)}) copy-start(f32[128,2]{0,1:T(2,128)} %param.11) | copy-start | bytes 3076
  108.0 18.9 %all-to-all-start.2 = ((bf16[64,8,128]{2,1,0:T(8,128)(2,1)}), bf16[64,8,128]{2,1,0:T(8,128)(2,1)S(1)}, u32[]{:S(2)}, u32[]{:S(2)}) async-start(bf16[64,8,128]{2,1,0:T(8,128)(2,1)} %back_rows.1), calls=%async_computation.2 | async-start | bytes 262144 | tf_op jit(solution)/shard_map/all_to_all | solution.py:431

commit v6 on v5

--- a/solution.py
+++ b/solution.py
@@ -58,31 +58,51 @@
 
 
 def send_kernel(
-    cap, at_s, me_s, tok_ref, grad_ref, act_ref, ids_ref, w_ref, out_ref, rank_s,
-    tok_v, grad_v, act_v, ids_s, w_s, seen_s, tok_t, grad_t, sems,
+    cap, at_s, me_s, tok_ref, grad_ref, act_ref, ids_ref, w_ref, out_ref, slot_s,
+    tok_v, grad_v, act_v, ids_s, w_s, next_s, tok_t, grad_t, sems,
 ):
     del me_s
     count, width = grad_ref.shape
-    experts = out_ref.shape[0]
+    block = 2 * cap + SHARED
+    experts = out_ref.shape[0] // block
     mine = pl.ds(pl.multiple_of((at_s[0] % 2) * HALF, HALF), HALF)
     line = pl.ds(pl.multiple_of((at_s[0] // 2) * LANES, LANES), LANES)
     pairs = (
-        (act_ref.at[:, line], act_v),
         (grad_ref, grad_v),
         (tok_ref.at[:, mine], tok_v),
         (ids_ref, ids_s),
         (w_ref, w_s),
+        (act_ref.at[:, line], act_v),
     )
     copies = [pltpu.make_async_copy(a, b, sems.at[i]) for i, (a, b) in enumerate(pairs)]
     for c in copies:
         c.start()
-    for e in range(experts):
-        seen_s[e] = 0
-    out_ref[:, : 2 * cap] = jnp.zeros((experts, 2 * cap, TILE, LANES), BF)
+
+    def clear(e, carry):
+        next_s[e] = e * block
+        out_ref[pl.ds(e * block, 2 * cap)] = jnp.zeros((2 * cap, TILE, LANES), BF)
+        return carry
+
+    lax.fori_loop(0, experts, clear, 0, unroll=4)
     for c in copies:
         c.wait()
     spread(tok_t, tok_v[...])
     spread(grad_t, grad_v[:, mine])
+
+    def one_token(t, carry):
+        rows = pl.ds(pl.multiple_of(t * TILE, TILE), TILE)
+        tok = tok_t[rows, :].astype(BF)
+        grad = grad_t[rows, :]
+        for k in range(2):
+            e = ids_s[k, t]
+            i = next_s[e]
+            next_s[e] = i + 1
+            slot_s[k, t] = i
+            out_ref[i] = tok
+            out_ref[i + cap] = (w_s[k, t] * grad).astype(BF)
+        return carry
+
+    lax.fori_loop(0, count, one_token, 0, unroll=8)
 
     half = LANES // 2
     act = act_v[...]
@@ -91,41 +111,26 @@
     keep = (iota(act.shape, 1) // half) * half == own
     twice = jnp.where(keep, act.astype(F32), swapped.astype(F32)).astype(BF)
     step = 2 * LANES
-    block = width // experts
-    n = step // block
-    steps = width // step
-
-    def one_step(i, carry):
-        for j in range(count // steps):
-            t = i * (count // steps) + j
-            rows = pl.ds(pl.multiple_of(t * TILE, TILE), TILE)
-            tok = tok_t[rows, :].astype(BF)
-            grad = grad_t[rows, :]
-            for k in range(2):
-                e = ids_s[k, t]
-                r = seen_s[e]
-                seen_s[e] = r + 1
-                rank_s[k, t] = r
-                out_ref[e, r] = tok
-                out_ref[e, cap + r] = (w_s[k, t] * grad).astype(BF)
-        cols = pl.ds(pl.multiple_of(i * step, step), step)
-        term = dot(grad_v[:, cols], twice, 0, 0).reshape(n, 2, block // 2, LANES)
-        left = iota((n, block // 2, LANES), 2) < half
+    cols = width // experts
+    for s in range(0, width, step):
+        term = dot(grad_v[:, s : s + step], twice, 0, 0)
+        term = term.reshape(step // cols, 2, cols // 2, LANES)
+        left = iota((step // cols, cols // 2, LANES), 2) < half
         both = jnp.where(left, term[:, 0], term[:, 1]).astype(BF)
-        out_ref[pl.ds(i * n, n), 2 * cap :] = both.reshape(n, SHARED, TILE, LANES)
-        return carry
-
-    lax.fori_loop(0, steps, one_step, 0)
+        for e in range(step // cols):
+            at = (s // cols + e) * block + 2 * cap
+            out_ref[at : at + SHARED] = both[e].reshape(SHARED, TILE, LANES)
 
 
 def send_rows(at, me, tokens, out_grad, act, ids_t, w_t, cap, experts):
     count, width = out_grad.shape
-    return pl.pallas_call(
+    block = 2 * cap + SHARED
+    sent, slots = pl.pallas_call(
         functools.partial(send_kernel, cap),
         in_specs=in_smem(2) + [pl.BlockSpec(memory_space=pltpu.HBM)] * 5,
         out_specs=in_vmem(1) + in_smem(1),
         out_shape=[
-            jax.ShapeDtypeStruct((experts, 2 * cap + SHARED, TILE, LANES), BF),
+            jax.ShapeDtypeStruct((experts * block, TILE, LANES), BF),
             jax.ShapeDtypeStruct((2, count), I32),
         ],
         scratch_shapes=[
@@ -142,6 +147,7 @@
         compiler_params=params(16),
         name="send_rows",
     )(at, me, tokens, out_grad, act, ids_t, w_t)
+    return sent.reshape(experts, block, TILE, LANES), slots
 
 
 def shared_kernel(cap, recv_ref, out_ref, norm_ref):
@@ -366,13 +372,14 @@
     )(parts, norms)
 
 
-def end_kernel(cap, me_s, recv_ref, ids_ref, rank_ref, w_ref, tok_ref, route_ref, norm_ref):
+def end_kernel(cap, me_s, recv_ref, ids_ref, slot_ref, w_ref, tok_ref, route_ref, norm_ref):
     n = recv_ref.shape[0]
     count = ids_ref.shape[1]
     rows = recv_ref[...].reshape(n * TILE, LANES)
     o = iota((n * TILE, count), 0)
-    first = [ids_ref[k : k + 1, :] * TILE for k in range(2)]
-    rank = [rank_ref[k : k + 1, :] for k in range(2)]
+    ids = [ids_ref[k : k + 1, :] for k in range(2)]
+    first = [i * TILE for i in ids]
+    rank = [slot_ref[k : k + 1, :] - ids[k] * (2 * cap + SHARED) for k in range(2)]
     pick = ones_at((o == first[0] + rank[0]) | (o == first[1] + rank[1]))
     tok_ref[...] = dot(pick, rows, 0, 0).astype(BF)
     route = []
@@ -386,7 +393,7 @@
     norm_ref[...] = sums[:1, : LANES // 2] + sums[:1, LANES // 2 :]
 
 
-def end(me, recv, ids_t, rank, w_t, cap):
+def end(me, recv, ids_t, slots, w_t, cap):
     count = ids_t.shape[1]
     return pl.pallas_call(
         functools.partial(end_kernel, cap),
@@ -399,7 +406,7 @@
         ],
         compiler_params=params(16),
         name="end",
-    )(me, recv, ids_t, rank, w_t)
+    )(me, recv, ids_t, slots, w_t)
 
 
 def swap(v):
@@ -415,7 +422,7 @@
     ids_t, w_t = expert_ids.T, route_weights.T
     here = (tokens, out_grad, shared_act, ids_t, w_t)
     here = [pltpu.with_memory_space_constraint(v, pltpu.HBM) for v in here]
-    sent, rank = send_rows(at, me, *here, cap, n)
+    sent, slots = send_rows(at, me, *here, cap, n)
     recv = lax.all_to_all(sent, EP, 0, 0, tiled=True)
     own = unpack(recv, cap)
     other = swap(own)
@@ -429,7 +436,7 @@
     back, hidden = lax.optimization_barrier((back, hidden))
     gate_grad, up_grad, down_grad, row_norms = grads(core, give, hidden, own, other)
     returned = lax.all_to_all(back, EP, 0, 0, tiled=True)
-    token_grad, route_grad, shared_norms = end(me, returned, ids_t, rank, w_t, cap)
+    token_grad, route_grad, shared_norms = end(me, returned, ids_t, slots, w_t, cap)
     return (
         token_grad,
         route_grad.T,

time: 129 us -> 129 us (level)
  no operation moved by 1% of the time
where the time goes in v6:
time: 129 us; the launch traced here: 128 us
  blocking collectives  89 us (69%)
  starting transfers between devices  16.8 us (13%)
  Pallas kernels  11 us (9%)
  waiting for transfers between devices  9.94 us (8%)
    all_to_all x1, blocking collectives, local(): recv = lax.all_to_all(sent, EP, 0, 0, tiled=True)  62.8 us
    all_to_all x1, blocking collectives, local(): back = back_rows(lax.all_to_all(part, 'x', 0, 0, tiled=True), norms, n, cap)  26.2 us
    all_to_all x1, waiting for transfers between devices, local(): returned = lax.all_to_all(back, EP, 0, 0, tiled=True)  9.68 us
    ppermute x3, starting transfers between devices, swap(): return lax.ppermute(v, 'c', [(0, 1), (1, 0)])  9.42 us
    all_to_all x1, starting transfers between devices, local(): returned = lax.all_to_all(back, EP, 0, 0, tiled=True)  7.4 us
    pallas_call x1, Pallas kernels, send_rows(): pl.pallas_call(functools.partial(send_kernel, cap), in_specs=in_smem(2) +...  3.48 us
  transfers between devices with their start and end apart: 4, of which 2 were waited for; matrix products, arithmetic and copies ran while one was open for 0% of the time, Pallas kernels for 3%

profile of v6, /device:TPU:1, one launch (start us, length us, event | category | flops | bytes accessed | tf_op | source)
XLA Modules:
  0.0 127.6 jit_solution(1970206716789537680)
XLA Ops:
  0.6 3.5 %send_rows.1 = (bf16[768,8,128]{2,1,0:T(8,128)(2,1)S(1)}, s32[2,128]{1,0:T(2,128)S(1)}) custom-call(s32[1]{0:T(128)} %bitcast.2.at_s, s32[1]{0:T(128)} %bitcast.me_s, bf16[128,2048]{1,0:T(8,128)(2,1)} %tok_ref.1, bf16[128,2048]{1,0:T(8,128)(2,1)} %grad_ref.1, bf16[128,1024]{1,0:T(8,128)(2,1)} %act_ref.1, s32[2,128]{1,0:T(2,128)} %bitcast.11, f32[2,128]{1,0:T(2,128)} %bitcast.13), custom_call_target="tpu_custom_call" | custom-call | tf_op jit(solution)/shard_map/send_rows/pallas_call | solution.py:128
  4.1 62.8 %all_to_all.15.recv_ref = bf16[64,12,8,128]{3,2,1,0:T(8,128)(2,1)S(1)} all-to-all(bf16[64,12,8,128]{3,2,1,0:T(8,128)(2,1)S(1)} %bitcast.10), channel_id=1, replica_groups=mesh['z'=8,'y'=8,'x'=8,'c'=2] {'z','y'}, dimensions={0} | all-to-all | bytes 3145728 | tf_op jit(solution)/shard_map/all_to_all | solution.py:426
  67.0 0.7 unpack.1.own_ref
  67.7 5.1 %collective-permute-start = (bf16[2,320,1024]{2,1,0:T(8,128)(2,1)S(1)}, bf16[2,320,1024]{2,1,0:T(8,128)(2,1)S(1)}, u32[]{:S(2)}, u32[]{:S(2)}) collective-permute-start(bf16[2,320,1024]{2,1,0:T(8,128)(2,1)S(1)} %unpack.1.own_ref), channel_id=1, source_target_pairs={{0,1},{1,0},{2,3},{3,2},{4,5},{5,4},{6,7},{7,6},{8,9},{9,8},{10,11... | collective-permute-start | bytes 3932168 | tf_op jit(solution)/shard_map/ppermute | solution.py:413
  72.8 0.0 copy-done
  72.8 0.0 copy-done.1
  72.8 0.0 copy-done.2
  72.8 0.8 half_products.1
  73.6 1.9 %collective-permute-start.2 = (bf16[256,1024]{1,0:T(8,128)(2,1)S(1)}, bf16[256,1024]{1,0:T(8,128)(2,1)S(1)}, u32[]{:S(2)}, u32[]{:S(2)}) collective-permute-start(bf16[256,1024]{1,0:T(8,128)(2,1)S(1)} %get-tuple-element.30), channel_id=1, source_target_pairs={{0,1},{1,0},{2,3},{3,2},{4,5},{5,4},{6,7},{7,6},{8,9},{9,8},{10,11... | collective-permute-start | bytes 1572872 | tf_op jit(solution)/shard_map/ppermute | solution.py:413
  75.5 0.0 collective-permute-done.other_ref
  75.5 0.8 forward.1
  76.4 2.4 %collective-permute-start.1 = (bf16[648,128]{1,0:T(8,128)(2,1)S(1)}, bf16[648,128]{1,0:T(8,128)(2,1)S(1)}, u32[]{:S(2)}, u32[]{:S(2)}) collective-permute-start(bf16[648,128]{1,0:T(8,128)(2,1)S(1)} %get-tuple-element.29.give_ref), channel_id=1, source_target_pairs={{0,1},{1,0},{2,3},{3,2},{4,5},{5,4},{6,7},{7,6},{8,9},{9,8},{10,11... | collective-permute-start | bytes 497672 | tf_op jit(solution)/shard_map/ppermute | solution.py:413
  78.8 0.8 shared_sum.1
  79.5 0.0 collective-permute-done.2.cols_ref
  79.5 0.3 collective-permute-done.1.take_ref
  79.8 0.9 shares.1
  80.7 26.2 %all_to_all.16.parts_ref = bf16[8,328,128]{2,1,0:T(8,128)(2,1)S(1)} all-to-all(bf16[8,328,128]{2,1,0:T(8,128)(2,1)S(1)} %shares.1), channel_id=1, replica_groups=mesh['z'=8,'y'=8,'x'=8,'c'=2] {'x'}, dimensions={0} | all-to-all | bytes 1343488 | tf_op jit(solution)/shard_map/all_to_all | solution.py:435
  106.9 0.8 back_rows.1
  107.7 7.4 %all-to-all-start.2 = ((bf16[64,8,128]{2,1,0:T(8,128)(2,1)}), bf16[64,8,128]{2,1,0:T(8,128)(2,1)S(1)}, u32[]{:S(2)}, u32[]{:S(2)}) async-start(bf16[64,8,128]{2,1,0:T(8,128)(2,1)} %back_rows.1), calls=%async_computation.2 | async-start | bytes 262144 | tf_op jit(solution)/shard_map/all_to_all | solution.py:438
  115.1 1.9 %grads.1 = (bf16[1,128,2048]{2,1,0:T(8,128)(2,1)}, bf16[1,128,2048]{2,1,0:T(8,128)(2,1)}, bf16[1,128,2048]{2,1,0:T(8,128)(2,1)}, f32[3,1,128]{2,1,0:T(1,128)}) custom-call(s32[1]{0:T(128)} %bitcast.1.core_s, bf16[648,128]{1,0:T(8,128)(2,1)S(1)} %get-tuple-element.29.give_ref, bf16[320,128]{1,0:T(8,128)(2,1)S(1)} %get-tuple-element.39.hidden_ref, ...), custom_call_target="tpu_custom_call" | custom-call | tf_op jit(solution)/shard_map/grads/pallas_call | solution.py:328
  117.0 9.7 %all-to-all-done.2.recv_ref = bf16[64,8,128]{2,1,0:T(8,128)(2,1)S(1)} async-done(((bf16[64,8,128]{2,1,0:T(8,128)(2,1)}), bf16[64,8,128]{2,1,0:T(8,128)(2,1)S(1)}, u32[]{:S(2)}, u32[]{:S(2)}) %all-to-all-start.2) | async-done | bytes 131104 | tf_op jit(solution)/shard_map/all_to_all | solution.py:438
  126.7 0.0 copy-done.3
  126.7 0.0 copy-done.4
  126.7 0.9 end.1
  (5 shorter events, 0.0 us)
Async XLA Ops:
  67.0 5.8 %copy-start = (bf16[1,128,2048]{2,1,0:T(8,128)(2,1)S(1)}, bf16[1,128,2048]{2,1,0:T(8,128)(2,1)}, u32[]{:S(2)}) copy-start(bf16[1,128,2048]{2,1,0:T(8,128)(2,1)} %gate_ref.5) | copy-start | bytes 1572868
  67.0 5.8 %copy-start.1 = (bf16[1,128,2048]{2,1,0:T(8,128)(2,1)S(1)}, bf16[1,128,2048]{2,1,0:T(8,128)(2,1)}, u32[]{:S(2)}) copy-start(bf16[1,128,2048]{2,1,0:T(8,128)(2,1)} %up_ref.5) | copy-start | bytes 1572868
  67.0 5.8 %copy-start.2 = (bf16[1,128,2048]{2,1,0:T(8,128)(2,1)S(1)}, bf16[1,128,2048]{2,1,0:T(8,128)(2,1)}, u32[]{:S(2)}) copy-start(bf16[1,128,2048]{2,1,0:T(8,128)(2,1)} %down_ref.3) | copy-start | bytes 1572868
  67.7 7.8 %collective-permute-start = (bf16[2,320,1024]{2,1,0:T(8,128)(2,1)S(1)}, bf16[2,320,1024]{2,1,0:T(8,128)(2,1)S(1)}, u32[]{:S(2)}, u32[]{:S(2)}) collective-permute-start(bf16[2,320,1024]{2,1,0:T(8,128)(2,1)S(1)} %unpack.1.own_ref), channel_id=1, source_target_pairs={{0,1},{1,0},{2,3},{3,2},{4,5},{5,4},{6,7},{7,6},{8,9},{9,8},{10,11... | collective-permute-start | bytes 3932168 | tf_op jit(solution)/shard_map/ppermute | solution.py:413
  73.6 6.0 %collective-permute-start.2 = (bf16[256,1024]{1,0:T(8,128)(2,1)S(1)}, bf16[256,1024]{1,0:T(8,128)(2,1)S(1)}, u32[]{:S(2)}, u32[]{:S(2)}) collective-permute-start(bf16[256,1024]{1,0:T(8,128)(2,1)S(1)} %get-tuple-element.30), channel_id=1, source_target_pairs={{0,1},{1,0},{2,3},{3,2},{4,5},{5,4},{6,7},{7,6},{8,9},{9,8},{10,11... | collective-permute-start | bytes 1572872 | tf_op jit(solution)/shard_map/ppermute | solution.py:413
  76.4 3.4 %collective-permute-start.1 = (bf16[648,128]{1,0:T(8,128)(2,1)S(1)}, bf16[648,128]{1,0:T(8,128)(2,1)S(1)}, u32[]{:S(2)}, u32[]{:S(2)}) collective-permute-start(bf16[648,128]{1,0:T(8,128)(2,1)S(1)} %get-tuple-element.29.give_ref), channel_id=1, source_target_pairs={{0,1},{1,0},{2,3},{3,2},{4,5},{5,4},{6,7},{7,6},{8,9},{9,8},{10,11... | collective-permute-start | bytes 497672 | tf_op jit(solution)/shard_map/ppermute | solution.py:413
  107.7 19.0 %copy-start.3 = (s32[128,2]{0,1:T(2,128)S(1)}, s32[128,2]{0,1:T(2,128)}, u32[]{:S(2)}) copy-start(s32[128,2]{0,1:T(2,128)} %param.10) | copy-start | bytes 3076
  107.7 19.0 %copy-start.4 = (f32[128,2]{0,1:T(2,128)S(1)}, f32[128,2]{0,1:T(2,128)}, u32[]{:S(2)}) copy-start(f32[128,2]{0,1:T(2,128)} %param.11) | copy-start | bytes 3076
  107.7 19.0 %all-to-all-start.2 = ((bf16[64,8,128]{2,1,0:T(8,128)(2,1)}), bf16[64,8,128]{2,1,0:T(8,128)(2,1)S(1)}, u32[]{:S(2)}, u32[]{:S(2)}) async-start(bf16[64,8,128]{2,1,0:T(8,128)(2,1)} %back_rows.1), calls=%async_computation.2 | async-start | bytes 262144 | tf_op jit(solution)/shard_map/all_to_all | solution.py:438
